TPU v7x, 512 devices: a whole 4x4x16 slice. The times are simulated.
512 devices in a mesh: sp: 32 (over z, core), tp: 16 (over y, x).
Axes of the slice: x: 4, y: 4, z: 16, core: 2. Of those that a mesh axis runs over, the one named last changes fastest.
Arguments:
- layer_input: bfloat16 [32768, 4096], P('sp', 'tp'), may hold values from -6 to 6
- key_weight: bfloat16 [4096, 4096], P(None, 'tp'), may hold values from -0.09375 to 0.09375
- value_weight: bfloat16 [4096, 4096], P(None, 'tp'), may hold values from -0.09375 to 0.09375
- decay_exponent: float32 [32], P('tp'), may hold values from -0.077 to -4.2114258e-05, as said below
- query_new: bfloat16 [2, 4096], P(None, 'tp'), may hold values from -6 to 6
- key_new: bfloat16 [2, 4096], P(None, 'tp'), may hold values from -6 to 6
- value_new: bfloat16 [2, 4096], P(None, 'tp'), may hold values from -6 to 6
- norm_gain: float32 [4096], P('tp'), may hold values from 0.1 to 1.9
Outputs:
- state_cache: bfloat16 [2, 32, 128, 128], P(None, 'tp', 'sp')
- first_read: bfloat16 [2, 4096], P(None, 'tp')
Inputs may be any that keep to these rules, and one draw needn't show every extreme that they name: decay_exponent is negative.
All inputs are finite; a program needn't handle non-finite values.
Results may differ from a plain program's by a relative error of at most 0.011.
Values may be sent and summed in bfloat16 or wider, within the bound.
A program may use at most 64 MiB of HBM per device.

v0:
```python
import jax
import jax.numpy as jnp
from jax import lax
from jax.sharding import PartitionSpec as P

SEQS = 2


def in_blocks(x, dim, peers):
    before, after = (x.shape[:dim], x.shape[dim + 1 :])
    return jnp.moveaxis(x.reshape(*before, peers, -1, *after), dim, 0)


def sent_and_summed(x, axis, dim):
    tiles = in_blocks(x, dim, lax.axis_size(axis))
    arrived = lax.all_to_all(tiles, axis, split_axis=0, concat_axis=0, tiled=True)
    return arrived.astype(jnp.float32).sum(axis=0)


def copy_for_each(x, axis):
    copies = jnp.broadcast_to(x, (lax.axis_size(axis), *x.shape))
    return lax.all_to_all(copies, axis, split_axis=0, concat_axis=0, tiled=True)


def of_everyone(x, axis):
    return copy_for_each(x, axis).sum(axis=0)


def rotate(projected, position):
    half_width = projected.shape[-1] // 2
    inverse = 1.0 / 10000.0 ** jnp.linspace(0.0, 1.0, half_width, dtype=jnp.float32)
    angle = position[:, None] * inverse[None, :]
    cosine = jnp.cos(angle)[:, None, :]
    sine = jnp.sin(angle)[:, None, :]
    first = projected[..., :half_width]
    second = projected[..., half_width:]
    return jnp.concatenate(
        [first * cosine - second * sine, first * sine + second * cosine], axis=-1
    )


def on_device(
    layer_input, key_weight, value_weight, decay_exponent, query_new, key_new, value_new, norm_gain
):
    tok_count = layer_input.shape[0]
    head_local = decay_exponent.shape[0]
    key_width = key_weight.shape[1] // head_local
    value_width = value_weight.shape[1] // head_local
    seq_span = lax.axis_size("sp") // SEQS
    seq_length = tok_count * seq_span
    sp_place = lax.axis_index("sp")
    feature_block = lax.all_gather(layer_input, "tp", axis=1, tiled=True)
    key_proj = jnp.dot(feature_block, key_weight, preferred_element_type=jnp.float32)
    value_proj = jnp.dot(feature_block, value_weight, preferred_element_type=jnp.float32)
    position = (sp_place % seq_span * tok_count + jnp.arange(tok_count, dtype=jnp.int32)).astype(
        jnp.float32
    )
    keys = (
        rotate(key_proj.reshape(tok_count, head_local, key_width), position) * key_width ** (-0.5)
    ).astype(jnp.bfloat16)
    values = value_proj.astype(jnp.bfloat16).reshape(tok_count, head_local, value_width)
    distance = seq_length - 1.0 - position
    weighting = jnp.exp(decay_exponent[None, :] * distance[:, None])
    weighted = (keys.astype(jnp.float32) * weighting[:, :, None]).astype(jnp.bfloat16)
    local_state = jnp.einsum("thd,the->hde", weighted, values, preferred_element_type=jnp.float32)
    member = (jnp.arange(SEQS, dtype=jnp.int32) == sp_place // seq_span).astype(jnp.float32)
    state_terms = member[:, None, None, None] * local_state[None]
    final_rows = sent_and_summed(state_terms.astype(jnp.bfloat16), "sp", 2)
    state_cache = final_rows.astype(jnp.bfloat16)
    queries = query_new.astype(jnp.float32).reshape(SEQS, head_local, key_width)
    partial_read = jnp.einsum(
        "shd,shde->she", queries, state_terms, precision=lax.Precision.HIGHEST
    )
    carried = of_everyone(partial_read, "sp")
    keys_next = key_new.astype(jnp.float32).reshape(SEQS, head_local, key_width)
    values_next = value_new.astype(jnp.float32).reshape(SEQS, head_local, value_width)
    own_term = jnp.sum(queries * keys_next, axis=2)[:, :, None] * values_next
    mixed = jnp.exp(decay_exponent)[None, :, None] * carried + own_term
    normed = mixed * lax.rsqrt(jnp.mean(mixed * mixed, axis=2, keepdims=True) + 1e-06)
    normed = normed * norm_gain.reshape(head_local, value_width)[None, :, :]
    return (state_cache, normed.reshape(SEQS, head_local * value_width).astype(jnp.bfloat16))


def solution(mesh):
    in_specs = (
        P("sp", "tp"),
        P(None, "tp"),
        P(None, "tp"),
        P("tp"),
        P(None, "tp"),
        P(None, "tp"),
        P(None, "tp"),
        P("tp"),
    )
    out_specs = (P(None, "tp", "sp", None), P(None, "tp"))
    return jax.shard_map(
        on_device, mesh=mesh, in_specs=in_specs, out_specs=out_specs, check_vma=False
    )
```

profile of v0, /device:TPU:1, one launch (start us, length us, event | category | flops | bytes accessed | tf_op | source)
XLA Modules:
  0.0 174.9 jit_solution(16979299565072083331)
XLA Ops:
  7.2 0.0 copy-start
  7.2 0.0 all-gather.2.cloned.1.call-start
  7.2 0.7 all-gather.2.cloned.1.call-update
  7.9 0.7 reshape.155
  8.6 0.7 exp.11
  9.3 0.1 fusion.12
  9.4 0.7 convert_multiply_fusion
  10.1 0.7 multiply_exponential_fusion
  10.8 1.0 multiply_cosine_fusion
  11.8 95.6 %all-gather.2.cloned.1.call-done = bf16[1024,4096]{1,0:T(8,128)(2,1)} async-done(((bf16[1024,256]{1,0:T(8,128)(2,1)}), bf16[1024,4096]{1,0:T(8,128)(2,1)}) %all-gather.2.cloned.1.call-update) | async-done | bytes 8388624 | tf_op jit(solution)/shard_map/all_gather | solution.py:52
  107.5 0.0 copy-done
  107.5 0.0 copy-start.3
  107.5 5.9 %fusion.15 = f32[1024,256]{0,1:T(8,128)S(1)} fusion(bf16[1024,4096]{1,0:T(8,128)(2,1)} %all-gather.2.cloned.1.call-done, bf16[4096,256]{1,0:T(8,128)(2,1)S(1)} %copy-done), kind=kOutput, calls=%fused_computation.37 | convolution fusion | flops 2147483648 | bytes 11534336 | tf_op jit(solution)/shard_map/dot_general | solution.py:53
  113.4 0.0 copy-start.4
  113.4 0.2 multiply_subtract_fusion
  113.5 0.0 copy-done.3
  113.6 1.4 copy-done.4
  115.0 2.4 %convolution_convert_fusion = bf16[1024,256]{0,1:T(8,128)(2,1)S(1)} fusion(bf16[1024,4096]{1,0:T(8,128)(2,1)S(1)} %copy-done.3, bf16[4096,256]{1,0:T(8,128)(2,1)S(1)} %copy-done.4), kind=kOutput, calls=%fused_computation | convolution fusion | flops 2147745792 | bytes 11010048 | tf_op jit(solution)/shard_map/dot_general | solution.py:54
  117.4 0.0 copy-start.1
  117.4 0.0 copy-start.2
  117.4 0.3 fusion.1
  117.7 0.3 fusion.5
  118.0 0.6 broadcast_in_dim.4
  118.7 14.4 %all-to-all-start.1 = ((f32[32,2,2,128]{3,2,1,0:T(2,128)}), f32[32,2,2,128]{3,2,1,0:T(2,128)S(1)}, u32[]{:S(2)}, u32[]{:S(2)}) async-start(f32[32,2,2,128]{3,2,1,0:T(2,128)} %broadcast_in_dim.4), calls=%async_computation.1 | async-start | bytes 131072 | tf_op jit(solution)/shard_map/all_to_all | solution.py:22
  133.1 0.1 broadcast_bitcast_fusion.2
  133.1 0.0 copy-done.1
  133.2 0.1 reduce_sum.44
  133.2 0.8 multiply_convert_fusion.2
  134.0 12.1 %all-to-all-done.1 = f32[32,2,2,128]{3,2,1,0:T(2,128)S(1)} async-done(((f32[32,2,2,128]{3,2,1,0:T(2,128)}), f32[32,2,2,128]{3,2,1,0:T(2,128)S(1)}, u32[]{:S(2)}, u32[]{:S(2)}) %all-to-all-start.1) | async-done | bytes 65568 | tf_op jit(solution)/shard_map/all_to_all | solution.py:22
  146.1 5.1 %all-to-all-start = ((bf16[32,2,2,4,128]{4,3,2,1,0:T(4,128)(2,1)}), bf16[32,2,2,4,128]{4,3,2,1,0:T(4,128)(2,1)S(1)}, u32[]{:S(2)}, u32[]{:S(2)}) async-start(bf16[32,2,2,4,128]{4,3,2,1,0:T(4,128)(2,1)} %multiply_convert_fusion.2), calls=%async_computation | async-start | bytes 262144 | tf_op jit(solution)/shard_map/all_to_all | solution.py:16
  151.2 0.2 broadcast_bitcast_fusion.1
  151.4 0.1 broadcast_bitcast_fusion
  151.5 0.0 copy-done.2
  151.5 0.6 fusion.10
  152.0 15.3 %all-to-all-done = bf16[32,2,2,4,128]{4,3,2,1,0:T(4,128)(2,1)S(1)} async-done(((bf16[32,2,2,4,128]{4,3,2,1,0:T(4,128)(2,1)}), bf16[32,2,2,4,128]{4,3,2,1,0:T(4,128)(2,1)S(1)}, u32[]{:S(2)}, u32[]{:S(2)}) %all-to-all-start) | async-done | bytes 131104 | tf_op jit(solution)/shard_map/all_to_all | solution.py:16
  167.4 0.7 reduce_sum.41
  (8 shorter events, 0.1 us)
Async XLA Ops:
  7.2 100.3 %copy-start = (bf16[4096,256]{1,0:T(8,128)(2,1)S(1)}, bf16[4096,256]{1,0:T(8,128)(2,1)}, u32[]{:S(2)}) copy-start(bf16[4096,256]{1,0:T(8,128)(2,1)} %param.9) | copy-start | bytes 6291460
  7.2 100.3 %all-gather.2.cloned.1.call-start = ((), (), s32[]{:S(2)}) async-start(), calls=%async_computation.2 | async-start | bytes 8912896 | tf_op jit(solution)/shard_map/all_gather | solution.py:52
  107.5 6.1 %copy-start.3 = (bf16[1024,4096]{1,0:T(8,128)(2,1)S(1)}, bf16[1024,4096]{1,0:T(8,128)(2,1)}, u32[]{:S(2)}) copy-start(bf16[1024,4096]{1,0:T(8,128)(2,1)} %all-gather.2.cloned.1.call-done) | copy-start | bytes 25165828
  113.4 1.6 copy-start.4
  117.4 15.8 %copy-start.1 = (bf16[2,256]{1,0:T(2,128)(2,1)S(1)}, bf16[2,256]{1,0:T(2,128)(2,1)}, u32[]{:S(2)}) copy-start(bf16[2,256]{1,0:T(2,128)(2,1)} %param.14) | copy-start | bytes 3076
  117.4 34.1 %copy-start.2 = (f32[256]{0:T(256)S(1)}, f32[256]{0:T(256)}, u32[]{:S(2)}) copy-start(f32[256]{0:T(256)} %param.15) | copy-start | bytes 3076
  118.7 27.4 %all-to-all-start.1 = ((f32[32,2,2,128]{3,2,1,0:T(2,128)}), f32[32,2,2,128]{3,2,1,0:T(2,128)S(1)}, u32[]{:S(2)}, u32[]{:S(2)}) async-start(f32[32,2,2,128]{3,2,1,0:T(2,128)} %broadcast_in_dim.4), calls=%async_computation.1 | async-start | bytes 131072 | tf_op jit(solution)/shard_map/all_to_all | solution.py:22
  146.1 21.3 %all-to-all-start = ((bf16[32,2,2,4,128]{4,3,2,1,0:T(4,128)(2,1)}), bf16[32,2,2,4,128]{4,3,2,1,0:T(4,128)(2,1)S(1)}, u32[]{:S(2)}, u32[]{:S(2)}) async-start(bf16[32,2,2,4,128]{4,3,2,1,0:T(4,128)(2,1)} %multiply_convert_fusion.2), calls=%async_computation | async-start | bytes 262144 | tf_op jit(solution)/shard_map/all_to_all | solution.py:16
Sparse Core Ops, SparseCore 0:
  11.0 96.4 all-gather.1
where the time goes:
time: 175 us
  waiting for transfers between devices  124 us (71%)
  starting transfers between devices  19.5 us (11%)
  between operations  14.2 us (8%)
  matrix products  8.92 us (5%)
  other arithmetic  4.99 us (3%)
  local copies, waits for them, and re-layouts  3.61 us (2%)
    all_gather x1, waiting for transfers between devices, on_device(): feature_block = lax.all_gather(layer_input, 'tp', axis=1, tiled=True)  95.6 us
    all_to_all x1, waiting for transfers between devices, sent_and_summed(): lax.all_to_all(tiles, axis, split_axis=0, concat_axis=0, tiled=True)  15.3 us
    all_to_all x1, starting transfers between devices, copy_for_each(): return lax.all_to_all(copies, axis, split_axis=0, concat_axis=0, tiled=True)  14.4 us
    all_to_all x1, waiting for transfers between devices, copy_for_each(): return lax.all_to_all(copies, axis, split_axis=0, concat_axis=0, tiled=True)  12.1 us
    dot_general x1, matrix products, on_device(): jnp.dot(feature_block, key_weight, preferred_element_type=jnp.float32)  5.9 us
    all_to_all x1, starting transfers between devices, sent_and_summed(): lax.all_to_all(tiles, axis, split_axis=0, concat_axis=0, tiled=True)  5.1 us
  transfers between devices with their start and end apart: 3, of which 3 were waited for; matrix products, arithmetic and copies ran while one was open for 3% of the time, Pallas kernels for 0%

commit v1 on v0

v1 whole, which is shorter than its diff:
```python
import jax
import jax.numpy as jnp
from jax import lax
from jax.experimental import pallas as pl
from jax.experimental.pallas import tpu as pltpu
from jax.sharding import PartitionSpec as P

MESH = pl.DeviceIdType.MESH
N = 4
TOK = 1024
FEAT = 256
PIECE = TOK // N
SP = 32
Z = 16

ORDER = [
    (0, 0), (1, 0), (2, 0), (3, 0),
    (1, 1), (2, 1), (2, 2), (3, 1), (3, 2), (3, 4),
    (2, 3), (3, 3), (3, 5), (3, 6),
    (3, 7),
]


def turn(mask, j):
    return ((mask << j) | (mask >> (N - j))) & (2**N - 1)


def select(d, values):
    total = 0
    for i, value in enumerate(values):
        if value:
            total = total + jnp.where(d == i, value, 0)
    return total


def flip1(v):
    return v + 1 - 2 * (v % 2)


def cos_sin(position, inverse):
    angle = position * inverse
    lane = lax.broadcasted_iota(jnp.int32, angle.shape, 1)
    quarter = jnp.floor(angle * 0.6366197723675814 + 0.5)
    rest = ((angle - quarter * 1.5703125) - quarter * 4.837512969970703125e-4) - quarter * 7.54978995489188e-8
    turns = quarter.astype(jnp.int32) - jnp.where(lane >= 64, 1, 0)
    turns = jnp.bitwise_and(turns, 3)
    square = rest * rest
    sine = rest + rest * square * (-1.6666654611e-1 + square * (8.3321608736e-3 - square * 1.9515295891e-4))
    cosine = 1.0 - 0.5 * square + square * square * (
        4.166664568298827e-2 + square * (-1.388731625493765e-3 + square * 2.443315711809948e-5)
    )
    value = jnp.where(jnp.bitwise_and(turns, 1) == 1, sine, cosine)
    negative = jnp.logical_or(turns == 1, turns == 2)
    return jnp.where(negative, -value, value)


def kernel(
    decay, x_hbm, wk_hbm, wv_hbm, query, key_new, value_new, gain, inverse,
    state_out, read_out,
    xbuf, wk, wv, acc, cosine, sine, weight, send_state, send_read, got_state, got_read,
    own_sem, w_sem, recv_sem, send_sem, tail_send, tail_send2, tail_recv, tail_recv2, self_sem, chain,
):
    sp = lax.axis_index("sp")
    tp = lax.axis_index("tp")
    z, core = sp // 2, sp % 2
    y, x = tp // 4, tp % 4
    links = [
        (sp, y * 4 + flip1(x)),
        (sp, y * 4 + 3 - x),
        (sp, flip1(y) * 4 + x),
        (sp, (3 - y) * 4 + x),
    ]
    sibling = (z * 2 + 1 - core, tp)

    def along_z(step):
        return ((z + step + Z) % Z * 2 + core, tp)

    def signal(semaphore, device):
        pl.semaphore_signal(semaphore, inc=1, device_id=device, device_id_type=MESH)

    own = [
        pltpu.make_async_copy(
            x_hbm.at[pl.ds(j * PIECE, PIECE)], xbuf.at[0, pl.ds(j * PIECE, PIECE)], own_sem.at[j]
        )
        for j in range(N)
    ]
    for copy in own:
        copy.start()
    wcopies = [
        pltpu.make_async_copy(wk_hbm, wk, w_sem.at[0]),
        pltpu.make_async_copy(wv_hbm, wv, w_sem.at[1]),
    ]
    for copy in wcopies:
        copy.start()

    barrier = pltpu.get_barrier_semaphore()
    near = links + [sibling, along_z(1), along_z(-1)]
    for device in near:
        signal(barrier, device)
    pl.semaphore_wait(barrier, len(near))

    def message(d, k, r):
        j = (d - k) % N
        m = turn(r, j)
        rows = pl.ds(j * PIECE, PIECE)
        arrives = m | (1 << d)
        return pltpu.make_async_remote_copy(
            src_ref=xbuf.at[m, rows],
            dst_ref=xbuf.at[arrives, rows],
            send_sem=send_sem,
            recv_sem=recv_sem.at[arrives, j],
            device_id=links[d],
            device_id_type=MESH,
        )

    for copy in own:
        copy.wait()
    for k, r in ORDER[:N]:
        for d in range(N):
            message(d, k, r).start()

    for j in range(N):
        rows = pl.ds(j * PIECE, PIECE)
        first = (sp % 16) * TOK + j * PIECE
        position = (
            lax.broadcasted_iota(jnp.int32, (PIECE, 128), 0) + first
        ).astype(jnp.float32)
        table = cos_sin(position, inverse[...])
        swapped = pltpu.roll(table, 64, axis=1)
        low = lax.broadcasted_iota(jnp.int32, (PIECE, 128), 1) < 64
        cosine[rows, :] = jnp.where(low, table, swapped)
        sine[rows, :] = jnp.where(low, -swapped, table)
        distance = 16384 - 1.0 - position
        for h in range(2):
            weight[h, rows, :] = jnp.exp(decay[h] * distance)

    for copy in wcopies:
        copy.wait()

    def column_of(m):
        b = [m // 2**i % 2 for i in range(N)]
        cx = x + b[0] * (1 - 2 * (x % 2))
        cx = cx + b[1] * (3 - 2 * cx)
        cy = y + b[2] * (1 - 2 * (y % 2))
        cy = cy + b[3] * (3 - 2 * cy)
        return cy * 4 + cx

    def add_product(m, j, first):
        t = column_of(m)
        wrows = pl.ds(pl.multiple_of(t * FEAT, FEAT), FEAT)
        rows = pl.ds(pl.multiple_of(j * PIECE, PIECE), PIECE)
        block = xbuf[m, rows, :]
        for i, w in enumerate((wk, wv)):
            part = jnp.dot(block, w[wrows, :], preferred_element_type=jnp.float32)
            if first:
                acc[i, rows, :] = part
            else:
                acc[i, rows, :] += part

    @pl.loop(0, N)
    def _(j):
        add_product(0, j, True)

    chain_steps = {0: [sibling, along_z(1), along_z(-1)], 2: [along_z(2), along_z(-2)],
                   4: [along_z(3), along_z(-3)], 6: [along_z(6), along_z(-6)]}
    pending = None

    for slot, (k, r) in enumerate(ORDER):
        for d in range(N):
            message(d, k, r).wait_recv()
        here = [q for q, (kk, rr) in enumerate(ORDER) if q >= N and forwards_after(kk, rr) == slot]
        for q in here:
            for d in range(N):
                message(d, *ORDER[q]).start()
        if slot in chain_steps:
            if pending is not None:
                pl.semaphore_wait(chain.at[pending[0]], pending[1])
            number = sorted(chain_steps).index(slot)
            for device in chain_steps[slot]:
                signal(chain.at[number], device)
            pending = (number, len(chain_steps[slot]))
        js = [(d - k) % N for d in range(N)]
        ms = [turn(r | (1 << k), j) for j in js]

        @pl.loop(0, N)
        def _(d):
            add_product(select(d, ms), select(d, js), False)

    pl.semaphore_wait(chain.at[pending[0]], pending[1])

    scale = 128 ** (-0.5)
    states = []
    for h in range(2):
        cols = pl.ds(h * 128, 128)
        k = acc[0, :, cols]
        turned = k * cosine[...] + pltpu.roll(k, 64, axis=1) * sine[...]
        keys = (turned * scale).astype(jnp.bfloat16)
        weighted = (keys.astype(jnp.float32) * weight[h]).astype(jnp.bfloat16)
        values = acc[1, :, cols].astype(jnp.bfloat16)
        states.append(
            lax.dot_general(
                weighted, values, (((0,), (0,)), ((), ())), preferred_element_type=jnp.float32
            )
        )
    top = lax.broadcasted_iota(jnp.int32, (8, 128), 0) < 4
    for i in range(16):
        a = states[0][8 * i : 8 * i + 8]
        b = states[1][8 * i : 8 * i + 8]
        send_state[2 * i] = jnp.where(top, a, pltpu.roll(b, 4, axis=0)).astype(jnp.bfloat16)
        send_state[2 * i + 1] = jnp.where(top, pltpu.roll(a, 4, axis=0), b).astype(jnp.bfloat16)
    prompt = z // 8
    for h in range(2):
        q = query[:, h * 128 : h * 128 + 128].astype(jnp.float32)
        both = jnp.dot(q, states[h], precision=lax.Precision.HIGHEST, preferred_element_type=jnp.float32)
        send_read[h : h + 1, :] = jnp.where(prompt == 0, both[0:1], both[1:2])

    def tail(step, other):
        target = (z + step + Z) % Z * 2 + (1 - core if other else core)
        state_copy = pltpu.make_async_remote_copy(
            src_ref=send_state.at[target], dst_ref=got_state.at[sp],
            send_sem=tail_send, recv_sem=tail_recv, device_id=(target, tp), device_id_type=MESH,
        )
        read_copy = pltpu.make_async_remote_copy(
            src_ref=send_read, dst_ref=got_read.at[sp],
            send_sem=tail_send2, recv_sem=tail_recv2, device_id=(target, tp), device_id_type=MESH,
        )
        return state_copy, read_copy

    steps = [8]
    for s in range(7, 0, -1):
        steps += [s, -s]
    for step in steps:
        for other in (False, True):
            for copy in tail(step, other):
                copy.start()
    for copy in tail(0, True):
        copy.start()
    pltpu.make_async_copy(send_state.at[sp], got_state.at[sp], tail_recv).start()
    pltpu.make_async_copy(send_read, got_read.at[sp], tail_recv2).start()

    queries = query[...].astype(jnp.float32)
    dots = queries * key_new[...].astype(jnp.float32)
    news = value_new[...].astype(jnp.float32)
    own_terms = [
        jnp.sum(dots[:, h * 128 : h * 128 + 128], axis=1, keepdims=True) * news[:, h * 128 : h * 128 + 128]
        for h in range(2)
    ]

    pltpu.make_async_copy(got_read, got_read, tail_recv2).wait()
    carried = [jnp.sum(got_read[16 * s : 16 * s + 16], axis=0) for s in range(2)]
    for h in range(2):
        scaled = jnp.exp(jnp.full((1, 128), decay[h], jnp.float32))
        rows = jnp.concatenate([carried[0][h : h + 1], carried[1][h : h + 1]], axis=0)
        mixed = scaled * rows + own_terms[h]
        normed = mixed * lax.rsqrt(jnp.mean(mixed * mixed, axis=1, keepdims=True) + 1e-06)
        read_out[:, h * 128 : h * 128 + 128] = normed * gain[:, h * 128 : h * 128 + 128]
    pltpu.make_async_copy(got_state, got_state, tail_recv).wait()
    for s in range(2):
        total = jnp.zeros((8, 128), jnp.float32)
        for i in range(16):
            total = total + got_state[16 * s + i].astype(jnp.float32)
        state_out[s] = total

    blocks = pl.ds(0, 15)
    pltpu.make_async_copy(xbuf.at[blocks], xbuf.at[blocks], send_sem).wait()
    others = pl.ds(0, SP - 1)
    pltpu.make_async_copy(got_state.at[others], got_state.at[others], tail_send).wait()
    pltpu.make_async_copy(got_read.at[others], got_read.at[others], tail_send2).wait()


def forwards_after(k, r):
    top = r.bit_length() - 1
    return ORDER.index((top, r - (1 << top)))


def on_device(
    layer_input, key_weight, value_weight, decay_exponent, query_new, key_new, value_new, norm_gain
):
    inverse = 1.0 / 10000.0 ** jnp.linspace(0.0, 1.0, 64, dtype=jnp.float32)
    inverse = jnp.concatenate([inverse, inverse])[None, :]
    vmem = pl.BlockSpec(memory_space=pltpu.VMEM)
    anywhere = pl.BlockSpec(memory_space=pl.ANY)
    state, read = pl.pallas_call(
        kernel,
        name="gather_project_reduce",
        out_shape=(
            jax.ShapeDtypeStruct((2, 8, 128), jnp.float32),
            jax.ShapeDtypeStruct((2, 256), jnp.float32),
        ),
        in_specs=[
            pl.BlockSpec(memory_space=pltpu.SMEM), anywhere, anywhere, anywhere,
            vmem, vmem, vmem, vmem, vmem,
        ],
        out_specs=(vmem, vmem),
        scratch_shapes=[
            pltpu.VMEM((16, TOK, FEAT), jnp.bfloat16),
            pltpu.VMEM((4096, 256), jnp.bfloat16),
            pltpu.VMEM((4096, 256), jnp.bfloat16),
            pltpu.VMEM((2, TOK, 256), jnp.float32),
            pltpu.VMEM((TOK, 128), jnp.float32),
            pltpu.VMEM((TOK, 128), jnp.float32),
            pltpu.VMEM((2, TOK, 128), jnp.float32),
            pltpu.VMEM((SP, 8, 128), jnp.bfloat16),
            pltpu.VMEM((2, 128), jnp.float32),
            pltpu.VMEM((SP, 8, 128), jnp.bfloat16),
            pltpu.VMEM((SP, 2, 128), jnp.float32),
            pltpu.SemaphoreType.DMA((N,)),
            pltpu.SemaphoreType.DMA((2,)),
            pltpu.SemaphoreType.DMA((16, N)),
            pltpu.SemaphoreType.DMA,
            pltpu.SemaphoreType.DMA,
            pltpu.SemaphoreType.DMA,
            pltpu.SemaphoreType.DMA,
            pltpu.SemaphoreType.DMA,
            pltpu.SemaphoreType.DMA,
            pltpu.SemaphoreType.REGULAR((4,)),
        ],
        compiler_params=pltpu.CompilerParams(collective_id=0, has_side_effects=True),
    )(
        decay_exponent, layer_input, key_weight, value_weight,
        query_new, key_new, value_new, norm_gain[None, :], inverse,
    )
    return (
        state.reshape(2, 2, 4, 128).astype(jnp.bfloat16),
        read.astype(jnp.bfloat16),
    )


def solution(mesh):
    in_specs = (
        P("sp", "tp"), P(None, "tp"), P(None, "tp"), P("tp"),
        P(None, "tp"), P(None, "tp"), P(None, "tp"), P("tp"),
    )
    out_specs = (P(None, "tp", "sp", None), P(None, "tp"))
    return jax.shard_map(
        on_device, mesh=mesh, in_specs=in_specs, out_specs=out_specs, check_vma=False
    )
```

time: 175 us -> 73.8 us (0.42)
  waiting for transfers between devices: 124 us -> 0 us
  Pallas kernels: 0 us -> 69.8 us
  starting transfers between devices: 19.5 us -> 0 us
  between operations: 14.2 us -> 0.64 us
  matrix products: 8.92 us -> 0 us
  local copies, waits for them, and re-layouts: 3.61 us -> 0 us
  other arithmetic: 4.99 us -> 3.19 us
    all_gather x1 -> x0, waiting for transfers between devices: 95.6 us -> none  [on_device(): feature_block = lax.all_gather(layer_input, 'tp', axis=1, tiled=True)]
    pallas_call x0 -> x1, Pallas kernels: none -> 69.8 us  [on_device(): pl.pallas_call(kernel, name='gather_project_reduce', out_shape=(jax.Shape...]
    all_to_all x2 -> x0, waiting for transfers between devices: 27.4 us -> none  [the longest x1 15.3 us: sent_and_summed(): lax.all_to_all(tiles, axis, split_axis=0, concat_axis=0, tiled=True)]
    all_to_all x2 -> x0, starting transfers between devices: 19.5 us -> none  [the longest x1 14.4 us: copy_for_each(): return lax.all_to_all(copies, axis, split_axis=0, concat_axis=0, tiled=True)]
    dot_general x4 -> x0, matrix products: 8.92 us -> none  [the longest x1 5.9 us: on_device(): jnp.dot(feature_block, key_weight, preferred_element_type=jnp.float32)]
  transfers between devices with their start and end apart: 3 -> 0, of which waited for: 3 -> 0; matrix products, arithmetic and copies ran while one was open for 3% -> 0% of each run, Pallas kernels for 0% -> 0%
where the time goes in v1:
time: 73.8 us; the launch traced here: 73.6 us
  Pallas kernels  69.8 us (95%)
  other arithmetic  3.19 us (4%)
    pallas_call x1, Pallas kernels, on_device(): pl.pallas_call(kernel, name='gather_project_reduce', out_shape=(jax.Shape...  69.8 us

profile of v1, /device:TPU:1, one launch (start us, length us, event | category | flops | bytes accessed | tf_op | source)
XLA Modules:
  0.0 73.6 jit_solution(9338624793107528750)
XLA Ops:
  0.6 0.1 fusion
  0.7 0.6 maximum_bitcast_fusion.inverse
  1.3 69.8 %gather_project_reduce.1 = (f32[2,8,128]{2,1,0:T(8,128)}, f32[2,256]{1,0:T(2,128)}) custom-call(f32[2]{0:T(128)} %decay.1, bf16[1024,256]{1,0:T(8,128)(2,1)} %x_hbm.1, bf16[4096,256]{1,0:T(8,128)(2,1)} %wk_hbm.1, bf16[4096,256]{1,0:T(8,128)(2,1)} %wv_hbm.1, bf16[2,256]{1,0:T(2,128)(2,1)} %query.1, bf16[2,256]{1,0:T(2,128)(2,1)} %key_new.1, ...), custom_call_target="tpu_custom_call" | custom-call | tf_op jit(solution)/shard_map/gather_project_reduce/pallas_call | solution.py:283
  71.1 1.3 %convert_element_type.9 = bf16[2,8,128]{2,1,0:T(8,128)(2,1)} convert(f32[2,8,128]{2,1,0:T(8,128)} %get-tuple-element.4) | non-fusion elementwise | flops 2048 | bytes 12288 | tf_op jit(solution)/shard_map/convert_element_type | solution.py:324
  72.4 1.2 %convert_element_type.11 = bf16[2,256]{1,0:T(2,128)(2,1)} convert(f32[2,256]{1,0:T(2,128)} %get-tuple-element.5) | non-fusion elementwise | flops 512 | bytes 3072 | tf_op jit(solution)/shard_map/convert_element_type | solution.py:325
  (1 shorter events, 0.0 us)

commit v2 on v1

v2 whole, which is shorter than its diff:
```python
import jax
import jax.numpy as jnp
import numpy as np
from jax import lax
from jax.experimental import pallas as pl
from jax.experimental.pallas import tpu as pltpu
from jax.sharding import PartitionSpec as P

MESH = pl.DeviceIdType.MESH
N = 3
TOK = 1024
FEAT = 256
STARTS = (0, 352, 688, 1024)
SP = 32
Z = 16

NATIVE_ORDER = [[(0, 0), (1, 0), (2, 0), (1, 1), (2, 1), (2, 2), (2, 3)]] * 3
FOREIGN_ORDER = [
    [(0, 0), (2, 0), (1, 0), (2, 1), (1, 1), (2, 2), (2, 3)],
    [(1, 0), (0, 0), (2, 0), (1, 1), (2, 1), (2, 2), (2, 3)],
    [(2, 0), (1, 0), (0, 0), (1, 1), (2, 1), (2, 2), (2, 3)],
]


def turn(mask, j):
    return ((mask << j) | (mask >> (N - j))) & (2**N - 1)


def piece(j):
    return pl.ds(STARTS[j], STARTS[j + 1] - STARTS[j])


def slot_messages(order, slot):
    out = []
    for d in range(N):
        k, r = order[d][slot]
        j = (d - k) % N
        out.append((d, j, turn(r, j), turn(r, j) | (1 << d)))
    return out


def onward(order, d, j, mask):
    out = []
    for dd in range(N):
        for slot in range(7):
            for link, jj, sent, _ in slot_messages(order, slot):
                if link == dd and jj == j and sent == mask:
                    out.append((slot, dd))
    return [dd for _, dd in sorted(out)]


def flip1(v):
    return v + 1 - 2 * (v % 2)


def cos_sin(position, inverse):
    angle = position * inverse
    lane = lax.broadcasted_iota(jnp.int32, angle.shape, 1)
    quarter = jnp.floor(angle * 0.6366197723675814 + 0.5)
    rest = ((angle - quarter * 1.5703125) - quarter * 4.837512969970703125e-4) - quarter * 7.54978995489188e-8
    turns = quarter.astype(jnp.int32) - jnp.where(lane >= 64, 1, 0)
    turns = jnp.bitwise_and(turns, 3)
    square = rest * rest
    sine = rest + rest * square * (-1.6666654611e-1 + square * (8.3321608736e-3 - square * 1.9515295891e-4))
    cosine = 1.0 - 0.5 * square + square * square * (
        4.166664568298827e-2 + square * (-1.388731625493765e-3 + square * 2.443315711809948e-5)
    )
    value = jnp.where(jnp.bitwise_and(turns, 1) == 1, sine, cosine)
    negative = jnp.logical_or(turns == 1, turns == 2)
    return jnp.where(negative, -value, value)


def kernel(
    decay, x_hbm, wk_hbm, wv_hbm, query, key_new, value_new, gain, inverse,
    state_out, read_out,
    xbuf, wk, wv, acc, cosine, sine, weight, mini_own, mini_got, send_state, send_read, got_state, got_read,
    mine_sem, sib_sem, w_sem, wl_sem, mini_sem,
    link_send, sib_send, x_send, w_send, wz_send, wzz_send, mini_send,
    tail_send, tail_send2, tail_recv, tail_recv2, chain,
):
    sp = lax.axis_index("sp")
    tp = lax.axis_index("tp")
    z, core = sp // 2, sp % 2
    y, x = tp // 4, tp % 4
    group = (x + 1) // 2 % 2
    block = z * 2 + group
    links = [
        (sp, y * 4 + 3 - x),
        (sp, flip1(y) * 4 + x),
        (sp, (3 - y) * 4 + x),
    ]
    sibling = (z * 2 + 1 - core, tp)
    partner_tp = y * 4 + flip1(x)
    partner = (z * 2 + 1 - core, partner_tp)

    def along_z(step):
        return ((z + step + Z) % Z * 2 + core, tp)

    def signal(semaphore, device):
        pl.semaphore_signal(semaphore, inc=1, device_id=device, device_id_type=MESH)

    def remote(src, dst, send, recv, device):
        return pltpu.make_async_remote_copy(
            src_ref=src, dst_ref=dst, send_sem=send, recv_sem=recv, device_id=device, device_id_type=MESH
        )

    def arrived(ref, semaphore):
        pltpu.make_async_copy(ref, ref, semaphore).wait()

    is_native = core == group
    is_foreign = core != group

    @pl.when(is_native)
    def _():
        for j in range(N):
            pltpu.make_async_copy(x_hbm.at[piece(j)], xbuf.at[0, 0, piece(j)], mine_sem.at[0, j]).start()
        pltpu.make_async_copy(wk_hbm, wk, wl_sem.at[0]).start()
        pltpu.make_async_copy(wv_hbm, wv, wl_sem.at[1]).start()

    for h in range(2):
        mini_own[h : h + 1, :] = jnp.full((1, 128), decay[h], jnp.float32)
        mini_own[2 + 2 * h : 4 + 2 * h, :] = query[:, h * 128 : h * 128 + 128].astype(jnp.float32)

    barrier = pltpu.get_barrier_semaphore()
    near = links + [sibling, partner, along_z(1), along_z(-1), along_z(2), along_z(-2)]
    for device in near:
        signal(barrier, device)
    pl.semaphore_wait(barrier, len(near))

    steps = [
        [sibling, partner, along_z(1), along_z(-1), along_z(2), along_z(-2)],
        [along_z(2), along_z(-2)],
        [sibling],
        [along_z(4), along_z(-4)],
    ]

    def chain_signal(n):
        for device in steps[n]:
            signal(chain.at[n], device)

    def chain_wait(n):
        pl.semaphore_wait(chain.at[n], len(steps[n]))

    def send_on(mask, j, over):
        for d in over:
            remote(
                xbuf.at[0, mask, piece(j)], xbuf.at[0, mask | (1 << d), piece(j)],
                link_send, mine_sem.at[mask | (1 << d), j], links[d],
            ).start()

    def to_sibling(mask, j):
        remote(
            xbuf.at[0, mask, piece(j)], xbuf.at[1, mask, piece(j)], sib_send, sib_sem.at[mask, j], sibling
        ).start()

    def column_of(mask, native_part):
        b = [mask // 2**i % 2 for i in range(N)]
        cx = x + b[0] * (3 - 2 * x)
        cy = y + b[1] * (1 - 2 * (y % 2))
        cy = cy + b[2] * (3 - 2 * cy)
        return cy * 4 + (cx if native_part else flip1(cx))

    def weight_rows(t):
        return pl.ds(pl.multiple_of(t * FEAT, FEAT), FEAT)

    def add_product(part, mask, j, native_part, first=False):
        wrows = weight_rows(column_of(mask, native_part))
        block_x = xbuf[part, mask, piece(j), :]
        for i, w in enumerate((wk, wv)):
            product = jnp.dot(block_x, w[wrows, :], preferred_element_type=jnp.float32)
            if first:
                acc[i, piece(j), :] = product
            else:
                acc[i, piece(j), :] += product

    def mine_arrived(mask, j):
        arrived(xbuf.at[0, mask, piece(j)], mine_sem.at[mask, j])

    def sib_arrived(mask, j):
        arrived(xbuf.at[1, mask, piece(j)], sib_sem.at[mask, j])

    def tables(mini):
        @pl.loop(0, 4)
        def _(c):
            rows = pl.ds(pl.multiple_of(c * 256, 256), 256)
            first = (block % 16) * TOK + c * 256
            position = (lax.broadcasted_iota(jnp.int32, (256, 128), 0) + first).astype(jnp.float32)
            table = cos_sin(position, inverse[...])
            swapped = pltpu.roll(table, 64, axis=1)
            low = lax.broadcasted_iota(jnp.int32, (256, 128), 1) < 64
            cosine[rows, :] = jnp.where(low, table, swapped)
            sine[rows, :] = jnp.where(low, -swapped, table)
            distance = 16384 - 1.0 - position
            for h in range(2):
                weight[h, rows, :] = jnp.exp(mini[h : h + 1, :] * distance)

    def receive_slot(order, slot):
        got = slot_messages(order, slot)
        for d, j, _, mask in got:
            mine_arrived(mask, j)
            send_on(mask, j, onward(order, d, j, mask))
            to_sibling(mask, j)
        return got

    @pl.when(is_native)
    def _():
        for j in range(N):
            mine_arrived(0, j)
        for slot in range(3):
            for d, j, mask, _ in slot_messages(NATIVE_ORDER, slot):
                send_on(mask, j, [d])
        for j in range(N):
            to_sibling(0, j)
        chain_signal(0)
        mini_got[...] = mini_own[...]
        tables(mini_own)
        arrived(wk, wl_sem.at[0])
        arrived(wv, wl_sem.at[1])
        for j in range(N):
            add_product(0, 0, j, True, first=True)
        for slot in range(7):
            got = receive_slot(NATIVE_ORDER, slot)
            if slot in (1, 3, 5):
                chain_wait(slot // 2)
                chain_signal(slot // 2 + 1)
            for _, j, _, mask in got:
                add_product(0, mask, j, True)
        for j in range(N):
            sib_arrived(0, j)
            add_product(1, 0, j, False)
        for slot in range(7):
            for _, j, _, mask in slot_messages(FOREIGN_ORDER, slot):
                sib_arrived(mask, j)
                add_product(1, mask, j, False)
        chain_wait(3)

    @pl.when(is_foreign)
    def _():
        quarter = z % 4
        opposite = (z + 2) % 4
        kv = ((wk_hbm, wk), (wv_hbm, wv))

        def direct(t):
            rows = weight_rows(t)
            for i, (src, dst) in enumerate(kv):
                remote(src.at[rows], dst.at[rows], w_send, w_sem.at[t, i], partner).start()

        def pass_weights(t, i, step, semaphore):
            ref = kv[i][1]
            rows = weight_rows(t)
            remote(ref.at[rows], ref.at[rows], semaphore, w_sem.at[t, i], along_z(step)).start()

        def exchange(j):
            remote(x_hbm.at[piece(j)], xbuf.at[0, 0, piece(j)], x_send, mine_sem.at[0, j], partner).start()

        def own_piece(j):
            mine_arrived(0, j)
            send_on(0, j, onward(FOREIGN_ORDER, 0, j, 0))
            to_sibling(0, j)

        def weights_arrived(t):
            for i, (_, ref) in enumerate(kv):
                arrived(ref.at[weight_rows(t)], w_sem.at[t, i])

        def own_weights(c):
            t = quarter * 4 + c
            weights_arrived(t)
            for i in range(2):
                pass_weights(t, i, 1, wz_send)
                pass_weights(t, i, -1, wz_send)
            if c == 0:
                pass_weights(t, 0, 2, wzz_send)
                pass_weights(t, 1, 2, wzz_send)
            if c == 1:
                pass_weights(t, 0, -2, wzz_send)
                pass_weights(t, 1, -2, wzz_send)
            if c == 3:
                pass_weights(t, 0, 2, wzz_send)
                pass_weights(t, 1, -2, wzz_send)

        def quarter_product(row, first=False):
            m1 = jnp.where(row == flip1(y), 2, 0)
            m2 = jnp.where(row == 3 - y, 4, 0)
            m3 = jnp.where(row == 3 - flip1(y), 6, 0)
            base = m1 + m2 + m3
            columns = (row * 4 + x, row * 4 + 3 - x)

            @pl.loop(0, 4)
            def _(c):
                rows = pl.ds(pl.multiple_of(c * 256, 256), 256)
                for i, w in enumerate((wk, wv)):
                    product = jnp.dot(
                        xbuf[1, base, rows, :], w[weight_rows(columns[0]), :], preferred_element_type=jnp.float32
                    ) + jnp.dot(
                        xbuf[1, base + 1, rows, :], w[weight_rows(columns[1]), :], preferred_element_type=jnp.float32
                    )
                    if first:
                        acc[i, rows, :] = product
                    else:
                        acc[i, rows, :] += product

        remote(mini_own, mini_got, mini_send, mini_sem, partner).start()
        exchange(0)
        direct(quarter * 4)
        exchange(1)
        exchange(2)
        for c in (1, 2, 3):
            direct(quarter * 4 + c)
        direct(opposite * 4 + 2)
        chain_signal(0)
        arrived(mini_got, mini_sem)
        tables(mini_got)
        own_piece(0)
        own_weights(0)
        chain_wait(0)
        chain_signal(1)
        own_piece(1)
        own_piece(2)
        receive_slot(FOREIGN_ORDER, 0)
        own_weights(1)
        chain_wait(1)
        chain_signal(2)
        own_weights(2)
        receive_slot(FOREIGN_ORDER, 1)
        own_weights(3)
        chain_wait(2)
        chain_signal(3)
        for mask in range(8):
            for j in range(N):
                sib_arrived(mask, j)
        quarter_product(quarter, first=True)
        receive_slot(FOREIGN_ORDER, 2)
        for step in (1, 3):
            row = (z + step) % 4
            for c in range(4):
                weights_arrived(row * 4 + c)
            quarter_product(row)
            receive_slot(FOREIGN_ORDER, 3 if step == 1 else 4)
        for c in range(4):
            weights_arrived(opposite * 4 + c)
        quarter_product(opposite)
        for j in range(N):
            add_product(0, 0, j, False)
        for slot in range(7):
            got = receive_slot(FOREIGN_ORDER, slot) if slot > 4 else slot_messages(FOREIGN_ORDER, slot)
            for _, j, _, mask in got:
                add_product(0, mask, j, False)
        chain_wait(3)

    scale = 128 ** (-0.5)
    states = []
    for h in range(2):
        cols = pl.ds(h * 128, 128)
        k = acc[0, :, cols]
        turned = k * cosine[...] + pltpu.roll(k, 64, axis=1) * sine[...]
        keys = (turned * scale).astype(jnp.bfloat16)
        weighted = (keys.astype(jnp.float32) * weight[h]).astype(jnp.bfloat16)
        values = acc[1, :, cols].astype(jnp.bfloat16)
        states.append(
            lax.dot_general(
                weighted, values, (((0,), (0,)), ((), ())), preferred_element_type=jnp.float32
            )
        )
    top = lax.broadcasted_iota(jnp.int32, (8, 128), 0) < 4
    for i in range(16):
        a = states[0][8 * i : 8 * i + 8]
        b = states[1][8 * i : 8 * i + 8]
        send_state[2 * i] = jnp.where(top, a, pltpu.roll(b, 4, axis=0)).astype(jnp.bfloat16)
        send_state[2 * i + 1] = jnp.where(top, pltpu.roll(a, 4, axis=0), b).astype(jnp.bfloat16)
    prompt = z // 8
    for h in range(2):
        rows = pl.ds(2 + 2 * h, 2)
        both = jnp.dot(mini_got[rows, :], states[h], precision=lax.Precision.HIGHEST, preferred_element_type=jnp.float32)
        send_read[h : h + 1, :] = jnp.where(prompt == 0, both[0:1], both[1:2])

    target_tp = jnp.where(is_native, tp, partner_tp)

    def tail(step, other):
        target = (z + step + Z) % Z * 2 + (1 - core if other else core)
        device = (target, target_tp)
        remote(send_state.at[target], got_state.at[block], tail_send, tail_recv, device).start()
        remote(send_read, got_read.at[block], tail_send2, tail_recv2, device).start()

    far = [8]
    for s in range(7, 0, -1):
        far += [s, -s]
    for step in far:
        for other in (False, True):
            tail(step, other)
    tail(0, True)

    @pl.when(is_native)
    def _():
        pltpu.make_async_copy(send_state.at[sp], got_state.at[block], tail_recv).start()
        pltpu.make_async_copy(send_read, got_read.at[block], tail_recv2).start()

    @pl.when(is_foreign)
    def _():
        tail(0, False)

    queries = query[...].astype(jnp.float32)
    dots = queries * key_new[...].astype(jnp.float32)
    news = value_new[...].astype(jnp.float32)
    own_terms = [
        jnp.sum(dots[:, h * 128 : h * 128 + 128], axis=1, keepdims=True) * news[:, h * 128 : h * 128 + 128]
        for h in range(2)
    ]

    arrived(got_read, tail_recv2)
    carried = [jnp.sum(got_read[16 * s : 16 * s + 16], axis=0) for s in range(2)]
    for h in range(2):
        scaled = jnp.exp(jnp.full((1, 128), decay[h], jnp.float32))
        rows = jnp.concatenate([carried[0][h : h + 1], carried[1][h : h + 1]], axis=0)
        mixed = scaled * rows + own_terms[h]
        normed = mixed * lax.rsqrt(jnp.mean(mixed * mixed, axis=1, keepdims=True) + 1e-06)
        read_out[:, h * 128 : h * 128 + 128] = normed * gain[:, h * 128 : h * 128 + 128]
    arrived(got_state, tail_recv)
    for s in range(2):
        total = jnp.zeros((8, 128), jnp.float32)
        for i in range(16):
            total = total + got_state[16 * s + i].astype(jnp.float32)
        state_out[s] = total

    arrived(xbuf.at[0, pl.ds(0, 7)], link_send)
    arrived(xbuf.at[0], sib_send)

    @pl.when(is_native)
    def _():
        arrived(got_state.at[pl.ds(0, 31)], tail_send)
        arrived(got_read.at[pl.ds(0, 31)], tail_send2)

    @pl.when(is_foreign)
    def _():
        arrived(got_state, tail_send)
        arrived(got_read, tail_send2)
        arrived(xbuf.at[0, 0], x_send)
        arrived(mini_own, mini_send)
        arrived(wk.at[pl.ds(0, 2560)], w_send)
        arrived(wk, wz_send)
        arrived(wk.at[pl.ds(0, 1536)], wzz_send)


def on_device(
    layer_input, key_weight, value_weight, decay_exponent, query_new, key_new, value_new, norm_gain
):
    inverse = (1.0 / 10000.0 ** (np.arange(64) / 63.0)).astype(np.float32)
    inverse = jnp.asarray(np.concatenate([inverse, inverse])[None, :])
    vmem = pl.BlockSpec(memory_space=pltpu.VMEM)
    anywhere = pl.BlockSpec(memory_space=pl.ANY)
    dma = pltpu.SemaphoreType.DMA
    state, read = pl.pallas_call(
        kernel,
        name="gather_project_reduce",
        out_shape=(
            jax.ShapeDtypeStruct((2, 8, 128), jnp.float32),
            jax.ShapeDtypeStruct((2, 256), jnp.float32),
        ),
        in_specs=[
            pl.BlockSpec(memory_space=pltpu.SMEM), anywhere, anywhere, anywhere,
            vmem, vmem, vmem, vmem, vmem,
        ],
        out_specs=(vmem, vmem),
        scratch_shapes=[
            pltpu.VMEM((2, 8, TOK, FEAT), jnp.bfloat16),
            pltpu.VMEM((4096, 256), jnp.bfloat16),
            pltpu.VMEM((4096, 256), jnp.bfloat16),
            pltpu.VMEM((2, TOK, 256), jnp.float32),
            pltpu.VMEM((TOK, 128), jnp.float32),
            pltpu.VMEM((TOK, 128), jnp.float32),
            pltpu.VMEM((2, TOK, 128), jnp.float32),
            pltpu.VMEM((8, 128), jnp.float32),
            pltpu.VMEM((8, 128), jnp.float32),
            pltpu.VMEM((SP, 8, 128), jnp.bfloat16),
            pltpu.VMEM((2, 128), jnp.float32),
            pltpu.VMEM((SP, 8, 128), jnp.bfloat16),
            pltpu.VMEM((SP, 2, 128), jnp.float32),
            dma((8, N)), dma((8, N)), dma((16, 2)), dma((2,)), dma,
            dma, dma, dma, dma, dma, dma, dma,
            dma, dma, dma, dma,
            pltpu.SemaphoreType.REGULAR((4,)),
        ],
        compiler_params=pltpu.CompilerParams(collective_id=0, has_side_effects=True),
    )(
        decay_exponent, layer_input, key_weight, value_weight,
        query_new, key_new, value_new, norm_gain[None, :], inverse,
    )
    return (
        state.reshape(2, 2, 4, 128).astype(jnp.bfloat16),
        read.astype(jnp.bfloat16),
    )


def solution(mesh):
    in_specs = (
        P("sp", "tp"), P(None, "tp"), P(None, "tp"), P("tp"),
        P(None, "tp"), P(None, "tp"), P(None, "tp"), P("tp"),
    )
    out_specs = (P(None, "tp", "sp", None), P(None, "tp"))
    return jax.shard_map(
        on_device, mesh=mesh, in_specs=in_specs, out_specs=out_specs, check_vma=False
    )
```

time: 73.8 us -> 66 us (0.89)
  Pallas kernels: 69.8 us -> 62.6 us
    pallas_call x1, Pallas kernels: 69.8 us -> 62.6 us  [on_device(): pl.pallas_call(kernel, name='gather_project_reduce', out_shape=(jax.Shape...]
where the time goes in v2:
time: 66 us; the launch traced here: 65.8 us
  Pallas kernels  62.6 us (95%)
  other arithmetic  2.51 us (4%)
    pallas_call x1, Pallas kernels, on_device(): pl.pallas_call(kernel, name='gather_project_reduce', out_shape=(jax.Shape...  62.6 us

profile of v2, /device:TPU:1, one launch (start us, length us, event | category | flops | bytes accessed | tf_op | source)
XLA Modules:
  0.0 65.8 jit_solution(2597534589471250883)
XLA Ops:
  0.6 62.6 %gather_project_reduce.1 = (f32[2,8,128]{2,1,0:T(8,128)}, f32[2,256]{1,0:T(2,128)}) custom-call(f32[2]{0:T(128)} %decay.1, bf16[1024,256]{1,0:T(8,128)(2,1)} %x_hbm.1, bf16[4096,256]{1,0:T(8,128)(2,1)} %wk_hbm.1, bf16[4096,256]{1,0:T(8,128)(2,1)} %wv_hbm.1, bf16[2,256]{1,0:T(2,128)(2,1)} %query.1, bf16[2,256]{1,0:T(2,128)(2,1)} %key_new.1, ...), custom_call_target="tpu_custom_call" | custom-call | tf_op jit(solution)/shard_map/gather_project_reduce/pallas_call | solution.py:451
  63.3 1.3 %convert_element_type.9 = bf16[2,8,128]{2,1,0:T(8,128)(2,1)} convert(f32[2,8,128]{2,1,0:T(8,128)} %get-tuple-element.4) | non-fusion elementwise | flops 2048 | bytes 12288 | tf_op jit(solution)/shard_map/convert_element_type | solution.py:488
  64.6 1.2 %convert_element_type.11 = bf16[2,256]{1,0:T(2,128)(2,1)} convert(f32[2,256]{1,0:T(2,128)} %get-tuple-element.5) | non-fusion elementwise | flops 512 | bytes 3072 | tf_op jit(solution)/shard_map/convert_element_type | solution.py:489

commit v3 on v2

--- a/solution.py
+++ b/solution.py
@@ -71,10 +71,11 @@
 
 
 def kernel(
-    decay, x_hbm, wk_hbm, wv_hbm, query, key_new, value_new, gain, inverse,
+    decay_hbm, x_hbm, wk_hbm, wv_hbm, query_hbm, key_hbm, value_hbm, gain_hbm, inverse_hbm,
     state_out, read_out,
+    decay, query, key_new, value_new, gain, inverse,
     xbuf, wk, wv, acc, cosine, sine, weight, mini_own, mini_got, send_state, send_read, got_state, got_read,
-    mine_sem, sib_sem, w_sem, wl_sem, mini_sem,
+    small_sem, mine_sem, sib_sem, w_sem, wl_sem, mini_sem,
     link_send, sib_send, x_send, w_send, wz_send, wzz_send, mini_send,
     tail_send, tail_send2, tail_recv, tail_recv2, chain,
 ):
@@ -110,21 +111,36 @@
     is_native = core == group
     is_foreign = core != group
 
-    @pl.when(is_native)
-    def _():
-        for j in range(N):
-            pltpu.make_async_copy(x_hbm.at[piece(j)], xbuf.at[0, 0, piece(j)], mine_sem.at[0, j]).start()
-        pltpu.make_async_copy(wk_hbm, wk, wl_sem.at[0]).start()
-        pltpu.make_async_copy(wv_hbm, wv, wl_sem.at[1]).start()
-
-    for h in range(2):
-        mini_own[h : h + 1, :] = jnp.full((1, 128), decay[h], jnp.float32)
-        mini_own[2 + 2 * h : 4 + 2 * h, :] = query[:, h * 128 : h * 128 + 128].astype(jnp.float32)
-
     barrier = pltpu.get_barrier_semaphore()
     near = links + [sibling, partner, along_z(1), along_z(-1), along_z(2), along_z(-2)]
     for device in near:
         signal(barrier, device)
+
+    @pl.when(is_native)
+    def _():
+        for j in range(N):
+            pltpu.make_async_copy(x_hbm.at[piece(j)], xbuf.at[0, 0, piece(j)], mine_sem.at[0, j]).start()
+
+    smalls = [
+        pltpu.make_async_copy(src, dst, small_sem.at[i])
+        for i, (src, dst) in enumerate((
+            (decay_hbm, decay), (query_hbm, query), (key_hbm, key_new), (value_hbm, value_new),
+            (gain_hbm, gain), (inverse_hbm, inverse),
+        ))
+    ]
+    for copy in smalls:
+        copy.start()
+
+    @pl.when(is_native)
+    def _():
+        pltpu.make_async_copy(wk_hbm, wk, wl_sem.at[0]).start()
+        pltpu.make_async_copy(wv_hbm, wv, wl_sem.at[1]).start()
+
+    for copy in smalls:
+        copy.wait()
+    for h in range(2):
+        mini_own[h : h + 1, :] = jnp.broadcast_to(decay[:, h : h + 1], (1, 128))
+        mini_own[2 + 2 * h : 4 + 2 * h, :] = query[:, h * 128 : h * 128 + 128].astype(jnp.float32)
     pl.semaphore_wait(barrier, len(near))
 
     steps = [
@@ -268,15 +284,6 @@
             for i in range(2):
                 pass_weights(t, i, 1, wz_send)
                 pass_weights(t, i, -1, wz_send)
-            if c == 0:
-                pass_weights(t, 0, 2, wzz_send)
-                pass_weights(t, 1, 2, wzz_send)
-            if c == 1:
-                pass_weights(t, 0, -2, wzz_send)
-                pass_weights(t, 1, -2, wzz_send)
-            if c == 3:
-                pass_weights(t, 0, 2, wzz_send)
-                pass_weights(t, 1, -2, wzz_send)
 
         def quarter_product(row, first=False):
             m1 = jnp.where(row == flip1(y), 2, 0)
@@ -299,27 +306,36 @@
                     else:
                         acc[i, rows, :] += product
 
+        def pass_on(step):
+            t = (z + step) % 4 * 4 + (1 if step == 1 else 0)
+            weights_arrived(t)
+            pass_weights(t, 0, -step, wzz_send)
+            pass_weights(t, 1, -step, wzz_send)
+
         remote(mini_own, mini_got, mini_send, mini_sem, partner).start()
-        exchange(0)
         direct(quarter * 4)
-        exchange(1)
-        exchange(2)
-        for c in (1, 2, 3):
+        direct(quarter * 4 + 1)
+        for j in range(N):
+            exchange(j)
+        for c in (2, 3):
             direct(quarter * 4 + c)
         direct(opposite * 4 + 2)
+        direct(opposite * 4 + 3)
         chain_signal(0)
+        own_weights(0)
+        own_weights(1)
+        chain_wait(0)
+        chain_signal(1)
+        own_piece(0)
+        pass_on(-1)
+        own_piece(1)
+        pass_on(1)
+        own_piece(2)
+        chain_wait(1)
+        chain_signal(2)
         arrived(mini_got, mini_sem)
         tables(mini_got)
-        own_piece(0)
-        own_weights(0)
-        chain_wait(0)
-        chain_signal(1)
-        own_piece(1)
-        own_piece(2)
         receive_slot(FOREIGN_ORDER, 0)
-        own_weights(1)
-        chain_wait(1)
-        chain_signal(2)
         own_weights(2)
         receive_slot(FOREIGN_ORDER, 1)
         own_weights(3)
@@ -330,12 +346,14 @@
                 sib_arrived(mask, j)
         quarter_product(quarter, first=True)
         receive_slot(FOREIGN_ORDER, 2)
+        receive_slot(FOREIGN_ORDER, 3)
         for step in (1, 3):
             row = (z + step) % 4
             for c in range(4):
-                weights_arrived(row * 4 + c)
+                if (step, c) not in ((1, 1), (3, 0)):
+                    weights_arrived(row * 4 + c)
             quarter_product(row)
-            receive_slot(FOREIGN_ORDER, 3 if step == 1 else 4)
+        receive_slot(FOREIGN_ORDER, 4)
         for c in range(4):
             weights_arrived(opposite * 4 + c)
         quarter_product(opposite)
@@ -409,7 +427,7 @@
     arrived(got_read, tail_recv2)
     carried = [jnp.sum(got_read[16 * s : 16 * s + 16], axis=0) for s in range(2)]
     for h in range(2):
-        scaled = jnp.exp(jnp.full((1, 128), decay[h], jnp.float32))
+        scaled = jnp.exp(mini_own[h : h + 1, :])
         rows = jnp.concatenate([carried[0][h : h + 1], carried[1][h : h + 1]], axis=0)
         mixed = scaled * rows + own_terms[h]
         normed = mixed * lax.rsqrt(jnp.mean(mixed * mixed, axis=1, keepdims=True) + 1e-06)
@@ -435,9 +453,9 @@
         arrived(got_read, tail_send2)
         arrived(xbuf.at[0, 0], x_send)
         arrived(mini_own, mini_send)
-        arrived(wk.at[pl.ds(0, 2560)], w_send)
+        arrived(wk.at[pl.ds(0, 3072)], w_send)
         arrived(wk, wz_send)
-        arrived(wk.at[pl.ds(0, 1536)], wzz_send)
+        arrived(wk.at[pl.ds(0, 1024)], wzz_send)
 
 
 def on_device(
@@ -452,15 +470,20 @@
         kernel,
         name="gather_project_reduce",
         out_shape=(
-            jax.ShapeDtypeStruct((2, 8, 128), jnp.float32),
-            jax.ShapeDtypeStruct((2, 256), jnp.float32),
+            pltpu.VMEM((2, 8, 128), jnp.float32),
+            pltpu.VMEM((2, 256), jnp.float32),
         ),
         in_specs=[
-            pl.BlockSpec(memory_space=pltpu.SMEM), anywhere, anywhere, anywhere,
-            vmem, vmem, vmem, vmem, vmem,
+            anywhere, anywhere, anywhere, anywhere, anywhere, anywhere, anywhere, anywhere, anywhere,
         ],
         out_specs=(vmem, vmem),
         scratch_shapes=[
+            pltpu.VMEM((1, 2), jnp.float32),
+            pltpu.VMEM((2, 256), jnp.bfloat16),
+            pltpu.VMEM((2, 256), jnp.bfloat16),
+            pltpu.VMEM((2, 256), jnp.bfloat16),
+            pltpu.VMEM((1, 256), jnp.float32),
+            pltpu.VMEM((1, 128), jnp.float32),
             pltpu.VMEM((2, 8, TOK, FEAT), jnp.bfloat16),
             pltpu.VMEM((4096, 256), jnp.bfloat16),
             pltpu.VMEM((4096, 256), jnp.bfloat16),
@@ -474,14 +497,14 @@
             pltpu.VMEM((2, 128), jnp.float32),
             pltpu.VMEM((SP, 8, 128), jnp.bfloat16),
             pltpu.VMEM((SP, 2, 128), jnp.float32),
-            dma((8, N)), dma((8, N)), dma((16, 2)), dma((2,)), dma,
+            dma((6,)), dma((8, N)), dma((8, N)), dma((16, 2)), dma((2,)), dma,
             dma, dma, dma, dma, dma, dma, dma,
             dma, dma, dma, dma,
             pltpu.SemaphoreType.REGULAR((4,)),
         ],
         compiler_params=pltpu.CompilerParams(collective_id=0, has_side_effects=True),
     )(
-        decay_exponent, layer_input, key_weight, value_weight,
+        decay_exponent[None, :], layer_input, key_weight, value_weight,
         query_new, key_new, value_new, norm_gain[None, :], inverse,
     )
     return (

time: 66 us -> 60.6 us (0.918)
  Pallas kernels: 62.6 us -> 58.7 us
  other arithmetic: 2.51 us -> 1.16 us
    pallas_call x1, Pallas kernels: 62.6 us -> 58.7 us  [on_device(): pl.pallas_call(kernel, name='gather_project_reduce', out_shape=(pltpu.VME...]
    convert_element_type x1, other arithmetic: 1.29 us -> 0.6 us  [on_device(): state.reshape(2, 2, 4, 128).astype(jnp.bfloat16)]
where the time goes in v3:
time: 60.6 us; the launch traced here: 60.5 us
  Pallas kernels  58.7 us (97%)
  other arithmetic  1.16 us (2%)
  between operations  0.64 us (1%)
    pallas_call x1, Pallas kernels, on_device(): pl.pallas_call(kernel, name='gather_project_reduce', out_shape=(pltpu.VME...  58.7 us

profile of v3, /device:TPU:1, one launch (start us, length us, event | category | flops | bytes accessed | tf_op | source)
XLA Modules:
  0.0 60.5 jit_solution(399325862606033552)
XLA Ops:
  0.6 58.7 %gather_project_reduce.1 = (f32[2,8,128]{2,1,0:T(8,128)S(1)}, f32[2,256]{1,0:T(2,128)S(1)}) custom-call(f32[1,2]{1,0:T(1,128)} %bitcast.5, bf16[1024,256]{1,0:T(8,128)(2,1)} %x_hbm.1, bf16[4096,256]{1,0:T(8,128)(2,1)} %wk_hbm.1, bf16[4096,256]{1,0:T(8,128)(2,1)} %wv_hbm.1, bf16[2,256]{1,0:T(2,128)(2,1)} %query_hbm.1, bf16[2,256]{1,0:T(2,128)(2,1)} %key_hbm.1, ...), custom_call_target="tpu_custom_call" | custom-call | tf_op jit(solution)/shard_map/gather_project_reduce/pallas_call | solution.py:469
  59.4 0.6 convert_element_type.9
  60.0 0.6 convert_element_type.11

commit v4 on v3

--- a/solution.py
+++ b/solution.py
@@ -14,12 +14,13 @@
 SP = 32
 Z = 16
 
-NATIVE_ORDER = [[(0, 0), (1, 0), (2, 0), (1, 1), (2, 1), (2, 2), (2, 3)]] * 3
-FOREIGN_ORDER = [
-    [(0, 0), (2, 0), (1, 0), (2, 1), (1, 1), (2, 2), (2, 3)],
-    [(1, 0), (0, 0), (2, 0), (1, 1), (2, 1), (2, 2), (2, 3)],
-    [(2, 0), (1, 0), (0, 0), (1, 1), (2, 1), (2, 2), (2, 3)],
-]
+NATIVE_ORDER = [(0, 0), (1, 0), (2, 0), (1, 1), (2, 1), (2, 2), (2, 3)]
+FOREIGN_OWN = [[(k, 0, j) for k in range(N)] for j in range(N)]
+FOREIGN_NEXT = [(1, 1, 0), (2, 1, 0), (2, 1, 1)]
+FOREIGN_THEN = [(1, 1, 1), (1, 1, 2), (2, 1, 2)]
+FOREIGN_LATE = [(2, 2, j) for j in range(N)]
+FOREIGN_LAST = [(2, 3, j) for j in range(N)]
+FOREIGN_ALL = FOREIGN_OWN + [FOREIGN_NEXT, FOREIGN_THEN, FOREIGN_LATE, FOREIGN_LAST]
 
 
 def turn(mask, j):
@@ -30,23 +31,19 @@
     return pl.ds(STARTS[j], STARTS[j + 1] - STARTS[j])
 
 
-def slot_messages(order, slot):
+def landing(k, r, j):
+    return turn(r, j) | (1 << (j + k) % N)
+
+
+def native_slot(slot):
+    k, r = NATIVE_ORDER[slot]
     out = []
     for d in range(N):
-        k, r = order[d][slot]
         j = (d - k) % N
-        out.append((d, j, turn(r, j), turn(r, j) | (1 << d)))
+        sent = r | (1 << k)
+        onward = [(j + kk) % N for kk, rr in NATIVE_ORDER if rr == sent]
+        out.append((j, turn(r, j), landing(k, r, j), onward))
     return out
-
-
-def onward(order, d, j, mask):
-    out = []
-    for dd in range(N):
-        for slot in range(7):
-            for link, jj, sent, _ in slot_messages(order, slot):
-                if link == dd and jj == j and sent == mask:
-                    out.append((slot, dd))
-    return [dd for _, dd in sorted(out)]
 
 
 def flip1(v):
@@ -83,7 +80,7 @@
     tp = lax.axis_index("tp")
     z, core = sp // 2, sp % 2
     y, x = tp // 4, tp % 4
-    group = (x + 1) // 2 % 2
+    group = 1 - (x + 1) // 2 % 2
     block = z * 2 + group
     links = [
         (sp, y * 4 + 3 - x),
@@ -136,12 +133,14 @@
         pltpu.make_async_copy(wk_hbm, wk, wl_sem.at[0]).start()
         pltpu.make_async_copy(wv_hbm, wv, wl_sem.at[1]).start()
 
-    for copy in smalls:
-        copy.wait()
-    for h in range(2):
-        mini_own[h : h + 1, :] = jnp.broadcast_to(decay[:, h : h + 1], (1, 128))
-        mini_own[2 + 2 * h : 4 + 2 * h, :] = query[:, h * 128 : h * 128 + 128].astype(jnp.float32)
     pl.semaphore_wait(barrier, len(near))
+
+    def fill_mini():
+        for copy in smalls:
+            copy.wait()
+        for h in range(2):
+            mini_own[h : h + 1, :] = jnp.broadcast_to(decay[:, h : h + 1], (1, 128))
+            mini_own[2 + 2 * h : 4 + 2 * h, :] = query[:, h * 128 : h * 128 + 128].astype(jnp.float32)
 
     steps = [
         [sibling, partner, along_z(1), along_z(-1), along_z(2), along_z(-2)],
@@ -210,44 +209,41 @@
             for h in range(2):
                 weight[h, rows, :] = jnp.exp(mini[h : h + 1, :] * distance)
 
-    def receive_slot(order, slot):
-        got = slot_messages(order, slot)
-        for d, j, _, mask in got:
-            mine_arrived(mask, j)
-            send_on(mask, j, onward(order, d, j, mask))
-            to_sibling(mask, j)
-        return got
-
     @pl.when(is_native)
     def _():
         for j in range(N):
             mine_arrived(0, j)
         for slot in range(3):
-            for d, j, mask, _ in slot_messages(NATIVE_ORDER, slot):
-                send_on(mask, j, [d])
+            for d in range(N):
+                send_on(0, (d - slot) % N, [d])
         for j in range(N):
             to_sibling(0, j)
         chain_signal(0)
+        fill_mini()
         mini_got[...] = mini_own[...]
-        tables(mini_own)
+        tables(mini_got)
         arrived(wk, wl_sem.at[0])
         arrived(wv, wl_sem.at[1])
         for j in range(N):
             add_product(0, 0, j, True, first=True)
         for slot in range(7):
-            got = receive_slot(NATIVE_ORDER, slot)
+            got = native_slot(slot)
+            for j, _, mask, onward in got:
+                mine_arrived(mask, j)
+                send_on(mask, j, onward)
+                to_sibling(mask, j)
             if slot in (1, 3, 5):
                 chain_wait(slot // 2)
                 chain_signal(slot // 2 + 1)
-            for _, j, _, mask in got:
+            for j, _, mask, _ in got:
                 add_product(0, mask, j, True)
         for j in range(N):
             sib_arrived(0, j)
             add_product(1, 0, j, False)
         for slot in range(7):
-            for _, j, _, mask in slot_messages(FOREIGN_ORDER, slot):
-                sib_arrived(mask, j)
-                add_product(1, mask, j, False)
+            for k, r, j in FOREIGN_ALL[slot]:
+                sib_arrived(landing(k, r, j), j)
+                add_product(1, landing(k, r, j), j, False)
         chain_wait(3)
 
     @pl.when(is_foreign)
@@ -271,8 +267,18 @@
 
         def own_piece(j):
             mine_arrived(0, j)
-            send_on(0, j, onward(FOREIGN_ORDER, 0, j, 0))
+            send_on(0, j, [(j + k) % N for k in range(N)])
             to_sibling(0, j)
+
+        def receive(k, r, j, *to):
+            mask = landing(k, r, j)
+            mine_arrived(mask, j)
+            send_on(mask, j, [(j + kk) % N for kk in to])
+            to_sibling(mask, j)
+
+        def foreign_product(messages):
+            for k, r, j in messages:
+                add_product(0, landing(k, r, j), j, False)
 
         def weights_arrived(t):
             for i, (_, ref) in enumerate(kv):
@@ -312,11 +318,12 @@
             pass_weights(t, 0, -step, wzz_send)
             pass_weights(t, 1, -step, wzz_send)
 
-        remote(mini_own, mini_got, mini_send, mini_sem, partner).start()
         direct(quarter * 4)
         direct(quarter * 4 + 1)
+        fill_mini()
         for j in range(N):
             exchange(j)
+        remote(mini_own, mini_got, mini_send, mini_sem, partner).start()
         for c in (2, 3):
             direct(quarter * 4 + c)
         direct(opposite * 4 + 2)
@@ -335,34 +342,53 @@
         chain_signal(2)
         arrived(mini_got, mini_sem)
         tables(mini_got)
-        receive_slot(FOREIGN_ORDER, 0)
+        receive(0, 0, 0, 1, 2)
+        receive(1, 0, 0)
+        receive(2, 0, 0)
         own_weights(2)
-        receive_slot(FOREIGN_ORDER, 1)
         own_weights(3)
+        receive(0, 0, 1, 1, 2)
+        receive(1, 0, 1)
+        send_on(landing(1, 0, 0), 0, [2])
+        receive(2, 0, 1)
         chain_wait(2)
         chain_signal(3)
+        receive(0, 0, 2, 1, 2)
+        send_on(landing(1, 0, 1), 1, [0])
+        receive(1, 0, 2, 2)
+        receive(2, 0, 2)
         for mask in range(8):
             for j in range(N):
                 sib_arrived(mask, j)
         quarter_product(quarter, first=True)
-        receive_slot(FOREIGN_ORDER, 2)
-        receive_slot(FOREIGN_ORDER, 3)
-        for step in (1, 3):
-            row = (z + step) % 4
-            for c in range(4):
-                if (step, c) not in ((1, 1), (3, 0)):
-                    weights_arrived(row * 4 + c)
-            quarter_product(row)
-        receive_slot(FOREIGN_ORDER, 4)
+        receive(1, 1, 0, 2)
+        receive(2, 1, 0)
+        receive(2, 1, 1)
+        row = (z + 1) % 4
+        for c in (0, 2, 3):
+            weights_arrived(row * 4 + c)
+        quarter_product(row)
         for c in range(4):
             weights_arrived(opposite * 4 + c)
+        row = (z + 3) % 4
+        for c in (1, 2, 3):
+            weights_arrived(row * 4 + c)
+        for j in range(N):
+            add_product(0, 0, j, False)
+        receive(1, 1, 1, 2)
+        receive(1, 1, 2, 2)
+        receive(2, 1, 2)
+        quarter_product(row)
+        foreign_product(FOREIGN_OWN[0])
+        foreign_product(FOREIGN_OWN[1])
+        for message in FOREIGN_LATE:
+            receive(*message)
         quarter_product(opposite)
-        for j in range(N):
-            add_product(0, 0, j, False)
-        for slot in range(7):
-            got = receive_slot(FOREIGN_ORDER, slot) if slot > 4 else slot_messages(FOREIGN_ORDER, slot)
-            for _, j, _, mask in got:
-                add_product(0, mask, j, False)
+        foreign_product(FOREIGN_OWN[2])
+        for message in FOREIGN_LAST:
+            receive(*message)
+        for messages in FOREIGN_ALL[3:]:
+            foreign_product(messages)
         chain_wait(3)
 
     scale = 128 ** (-0.5)

time: 60.6 us -> 59 us (0.974)
  Pallas kernels: 58.7 us -> 57.1 us
    pallas_call x1, Pallas kernels: 58.7 us -> 57.1 us  [on_device(): pl.pallas_call(kernel, name='gather_project_reduce', out_shape=(pltpu.VME...]
where the time goes in v4:
time: 59 us; the launch traced here: 58.9 us
  Pallas kernels  57.1 us (97%)
  other arithmetic  1.16 us (2%)
  between operations  0.64 us (1%)
    pallas_call x1, Pallas kernels, on_device(): pl.pallas_call(kernel, name='gather_project_reduce', out_shape=(pltpu.VME...  57.1 us

profile of v4, /device:TPU:1, one launch (start us, length us, event | category | flops | bytes accessed | tf_op | source)
XLA Modules:
  0.0 58.9 jit_solution(13808644907573245753)
XLA Ops:
  0.6 57.1 %gather_project_reduce.1 = (f32[2,8,128]{2,1,0:T(8,128)S(1)}, f32[2,256]{1,0:T(2,128)S(1)}) custom-call(f32[1,2]{1,0:T(1,128)} %bitcast.5, bf16[1024,256]{1,0:T(8,128)(2,1)} %x_hbm.1, bf16[4096,256]{1,0:T(8,128)(2,1)} %wk_hbm.1, bf16[4096,256]{1,0:T(8,128)(2,1)} %wv_hbm.1, bf16[2,256]{1,0:T(2,128)(2,1)} %query_hbm.1, bf16[2,256]{1,0:T(2,128)(2,1)} %key_hbm.1, ...), custom_call_target="tpu_custom_call" | custom-call | tf_op jit(solution)/shard_map/gather_project_reduce/pallas_call | solution.py:495
  57.8 0.6 %convert_element_type.9 = bf16[2,8,128]{2,1,0:T(8,128)(2,1)} convert(f32[2,8,128]{2,1,0:T(8,128)S(1)} %get-tuple-element.4) | non-fusion elementwise | flops 2048 | bytes 12288 | tf_op jit(solution)/shard_map/convert_element_type | solution.py:537
  58.4 0.6 convert_element_type.11

commit v5 on v4

--- a/solution.py
+++ b/solution.py
@@ -15,12 +15,7 @@
 Z = 16
 
 NATIVE_ORDER = [(0, 0), (1, 0), (2, 0), (1, 1), (2, 1), (2, 2), (2, 3)]
-FOREIGN_OWN = [[(k, 0, j) for k in range(N)] for j in range(N)]
-FOREIGN_NEXT = [(1, 1, 0), (2, 1, 0), (2, 1, 1)]
-FOREIGN_THEN = [(1, 1, 1), (1, 1, 2), (2, 1, 2)]
-FOREIGN_LATE = [(2, 2, j) for j in range(N)]
-FOREIGN_LAST = [(2, 3, j) for j in range(N)]
-FOREIGN_ALL = FOREIGN_OWN + [FOREIGN_NEXT, FOREIGN_THEN, FOREIGN_LATE, FOREIGN_LAST]
+FOREIGN_ORDER = [(0, 0), (1, 0), (1, 1), (2, 0), (2, 1), (2, 2), (2, 3)]
 
 
 def turn(mask, j):
@@ -241,7 +236,8 @@
             sib_arrived(0, j)
             add_product(1, 0, j, False)
         for slot in range(7):
-            for k, r, j in FOREIGN_ALL[slot]:
+            k, r = FOREIGN_ORDER[slot]
+            for j in range(N):
                 sib_arrived(landing(k, r, j), j)
                 add_product(1, landing(k, r, j), j, False)
         chain_wait(3)
@@ -252,10 +248,15 @@
         opposite = (z + 2) % 4
         kv = ((wk_hbm, wk), (wv_hbm, wv))
 
-        def direct(t):
+        other = flip1(x)
+        mine_first = (x, 3 - x, other, 3 - other)
+        theirs_first = (other, 3 - other, x, 3 - x)
+
+        def direct(row, i):
+            t = row * 4 + theirs_first[i]
             rows = weight_rows(t)
-            for i, (src, dst) in enumerate(kv):
-                remote(src.at[rows], dst.at[rows], w_send, w_sem.at[t, i], partner).start()
+            for n, (src, dst) in enumerate(kv):
+                remote(src.at[rows], dst.at[rows], w_send, w_sem.at[t, n], partner).start()
 
         def pass_weights(t, i, step, semaphore):
             ref = kv[i][1]
@@ -267,7 +268,7 @@
 
         def own_piece(j):
             mine_arrived(0, j)
-            send_on(0, j, [(j + k) % N for k in range(N)])
+            send_on(0, j, [j])
             to_sibling(0, j)
 
         def receive(k, r, j, *to):
@@ -276,58 +277,46 @@
             send_on(mask, j, [(j + kk) % N for kk in to])
             to_sibling(mask, j)
 
-        def foreign_product(messages):
-            for k, r, j in messages:
+        def native_product(slot):
+            for j, _, mask, _ in native_slot(slot):
+                sib_arrived(mask, j)
+                add_product(1, mask, j, True)
+
+        def foreign_product(k, r):
+            for j in range(N):
                 add_product(0, landing(k, r, j), j, False)
 
         def weights_arrived(t):
             for i, (_, ref) in enumerate(kv):
                 arrived(ref.at[weight_rows(t)], w_sem.at[t, i])
 
-        def own_weights(c):
-            t = quarter * 4 + c
+        def own_weights(i):
+            t = quarter * 4 + mine_first[i]
             weights_arrived(t)
-            for i in range(2):
-                pass_weights(t, i, 1, wz_send)
-                pass_weights(t, i, -1, wz_send)
-
-        def quarter_product(row, first=False):
-            m1 = jnp.where(row == flip1(y), 2, 0)
-            m2 = jnp.where(row == 3 - y, 4, 0)
-            m3 = jnp.where(row == 3 - flip1(y), 6, 0)
-            base = m1 + m2 + m3
-            columns = (row * 4 + x, row * 4 + 3 - x)
-
-            @pl.loop(0, 4)
-            def _(c):
-                rows = pl.ds(pl.multiple_of(c * 256, 256), 256)
-                for i, w in enumerate((wk, wv)):
-                    product = jnp.dot(
-                        xbuf[1, base, rows, :], w[weight_rows(columns[0]), :], preferred_element_type=jnp.float32
-                    ) + jnp.dot(
-                        xbuf[1, base + 1, rows, :], w[weight_rows(columns[1]), :], preferred_element_type=jnp.float32
-                    )
-                    if first:
-                        acc[i, rows, :] = product
-                    else:
-                        acc[i, rows, :] += product
+            for n in range(2):
+                pass_weights(t, n, 1, wz_send)
+                pass_weights(t, n, -1, wz_send)
 
         def pass_on(step):
-            t = (z + step) % 4 * 4 + (1 if step == 1 else 0)
+            t = (z + step) % 4 * 4 + mine_first[1 if step == 1 else 0]
             weights_arrived(t)
             pass_weights(t, 0, -step, wzz_send)
             pass_weights(t, 1, -step, wzz_send)
 
-        direct(quarter * 4)
-        direct(quarter * 4 + 1)
+        def row_weights(step, *indices):
+            for i in indices:
+                weights_arrived((z + step) % 4 * 4 + mine_first[i])
+
+        direct(quarter, 0)
+        direct(quarter, 1)
         fill_mini()
         for j in range(N):
             exchange(j)
         remote(mini_own, mini_got, mini_send, mini_sem, partner).start()
-        for c in (2, 3):
-            direct(quarter * 4 + c)
-        direct(opposite * 4 + 2)
-        direct(opposite * 4 + 3)
+        direct(quarter, 2)
+        direct(quarter, 3)
+        direct(opposite, 2)
+        direct(opposite, 3)
         chain_signal(0)
         own_weights(0)
         own_weights(1)
@@ -336,59 +325,62 @@
         own_piece(0)
         pass_on(-1)
         own_piece(1)
+        send_on(0, 0, [1])
         pass_on(1)
         own_piece(2)
+        send_on(0, 1, [2])
+        send_on(0, 2, [0])
         chain_wait(1)
         chain_signal(2)
         arrived(mini_got, mini_sem)
         tables(mini_got)
-        receive(0, 0, 0, 1, 2)
-        receive(1, 0, 0)
-        receive(2, 0, 0)
+        receive(0, 0, 0, 1)
+        row_weights(1, 0)
+        row_weights(3, 1)
+        row_weights(2, 0, 1)
+        for j in range(N):
+            sib_arrived(0, j)
+            add_product(1, 0, j, True, first=True)
         own_weights(2)
+        native_product(0)
+        receive(0, 0, 1, 1)
+        native_product(1)
+        native_product(2)
         own_weights(3)
-        receive(0, 0, 1, 1, 2)
-        receive(1, 0, 1)
-        send_on(landing(1, 0, 0), 0, [2])
-        receive(2, 0, 1)
+        receive(0, 0, 2, 1)
+        for j in range(N):
+            send_on(0, j, [(j + 2) % N])
+            send_on(landing(0, 0, j), j, [(j + 2) % N])
         chain_wait(2)
         chain_signal(3)
-        receive(0, 0, 2, 1, 2)
-        send_on(landing(1, 0, 1), 1, [0])
-        receive(1, 0, 2, 2)
-        receive(2, 0, 2)
-        for mask in range(8):
-            for j in range(N):
-                sib_arrived(mask, j)
-        quarter_product(quarter, first=True)
-        receive(1, 1, 0, 2)
-        receive(2, 1, 0)
-        receive(2, 1, 1)
-        row = (z + 1) % 4
-        for c in (0, 2, 3):
-            weights_arrived(row * 4 + c)
-        quarter_product(row)
-        for c in range(4):
-            weights_arrived(opposite * 4 + c)
-        row = (z + 3) % 4
-        for c in (1, 2, 3):
-            weights_arrived(row * 4 + c)
+        native_product(3)
+        native_product(4)
+        for j in (2, 0, 1):
+            receive(1, 0, j, 2)
+        native_product(5)
+        native_product(6)
+        for j in range(N):
+            receive(1, 1, j, 2)
+        for j in range(N):
+            receive(2, 0, j)
+        row_weights(1, 2, 3)
+        row_weights(3, 2, 3)
+        row_weights(2, 2, 3)
         for j in range(N):
             add_product(0, 0, j, False)
-        receive(1, 1, 1, 2)
-        receive(1, 1, 2, 2)
-        receive(2, 1, 2)
-        quarter_product(row)
-        foreign_product(FOREIGN_OWN[0])
-        foreign_product(FOREIGN_OWN[1])
-        for message in FOREIGN_LATE:
-            receive(*message)
-        quarter_product(opposite)
-        foreign_product(FOREIGN_OWN[2])
-        for message in FOREIGN_LAST:
-            receive(*message)
-        for messages in FOREIGN_ALL[3:]:
-            foreign_product(messages)
+        foreign_product(0, 0)
+        foreign_product(1, 0)
+        for j in range(N):
+            receive(2, 1, j)
+        foreign_product(1, 1)
+        foreign_product(2, 0)
+        for j in range(N):
+            receive(2, 2, j)
+        foreign_product(2, 1)
+        foreign_product(2, 2)
+        for j in range(N):
+            receive(2, 3, j)
+        foreign_product(2, 3)
         chain_wait(3)
 
     scale = 128 ** (-0.5)

time: 59 us -> 59.2 us (level)
  no operation moved by 1% of the time
where the time goes in v5:
time: 59.2 us; the launch traced here: 59.1 us
  Pallas kernels  57.3 us (97%)
  other arithmetic  1.16 us (2%)
  between operations  0.64 us (1%)
    pallas_call x1, Pallas kernels, on_device(): pl.pallas_call(kernel, name='gather_project_reduce', out_shape=(pltpu.VME...  57.3 us

profile of v5, /device:TPU:1, one launch (start us, length us, event | category | flops | bytes accessed | tf_op | source)
XLA Modules:
  0.0 59.1 jit_solution(6657373102605679600)
XLA Ops:
  0.6 57.3 %gather_project_reduce.1 = (f32[2,8,128]{2,1,0:T(8,128)S(1)}, f32[2,256]{1,0:T(2,128)S(1)}) custom-call(f32[1,2]{1,0:T(1,128)} %bitcast.5, bf16[1024,256]{1,0:T(8,128)(2,1)} %x_hbm.1, bf16[4096,256]{1,0:T(8,128)(2,1)} %wk_hbm.1, bf16[4096,256]{1,0:T(8,128)(2,1)} %wv_hbm.1, bf16[2,256]{1,0:T(2,128)(2,1)} %query_hbm.1, bf16[2,256]{1,0:T(2,128)(2,1)} %key_hbm.1, ...), custom_call_target="tpu_custom_call" | custom-call | tf_op jit(solution)/shard_map/gather_project_reduce/pallas_call | solution.py:487
  57.9 0.6 %convert_element_type.9 = bf16[2,8,128]{2,1,0:T(8,128)(2,1)} convert(f32[2,8,128]{2,1,0:T(8,128)S(1)} %get-tuple-element.4) | non-fusion elementwise | flops 2048 | bytes 12288 | tf_op jit(solution)/shard_map/convert_element_type | solution.py:529
  58.5 0.6 convert_element_type.11

commit v6 on v5

--- a/solution.py
+++ b/solution.py
@@ -15,7 +15,24 @@
 Z = 16
 
 NATIVE_ORDER = [(0, 0), (1, 0), (2, 0), (1, 1), (2, 1), (2, 2), (2, 3)]
-FOREIGN_ORDER = [(0, 0), (1, 0), (1, 1), (2, 0), (2, 1), (2, 2), (2, 3)]
+FOREIGN_ORDER = [
+    (0, 0, 0), (0, 0, 1), (1, 0, 2), (0, 0, 2), (1, 0, 0), (2, 0, 1), (1, 0, 1), (1, 1, 0), (2, 1, 1), (2, 0, 0),
+    (2, 0, 2), (1, 1, 2), (1, 1, 1), (2, 1, 2), (2, 2, 1), (2, 1, 0), (2, 2, 2), (2, 2, 0), (2, 3, 1), (2, 3, 2),
+    (2, 3, 0),
+]
+OWN_SENDS = [
+    [(0, 0, 0)],
+    [(0, 0, 1), (1, 0, 0)],
+    [(0, 0, 2), (1, 0, 1), (1, 0, 2), (2, 0, 1), (2, 0, 0)],
+]
+SENDS = {
+    (0, 0, 0): [(1, 1, 0), (2, 0, 2)],
+    (0, 0, 1): [(1, 1, 1), (2, 1, 1), (2, 1, 0)],
+    (0, 0, 2): [(1, 1, 2), (2, 1, 2)],
+}
+for _j in range(N):
+    SENDS[1, 0, _j] = [(2, 2, _j)]
+    SENDS[1, 1, _j] = [(2, 3, _j)]
 
 
 def turn(mask, j):
@@ -66,7 +83,7 @@
     decay_hbm, x_hbm, wk_hbm, wv_hbm, query_hbm, key_hbm, value_hbm, gain_hbm, inverse_hbm,
     state_out, read_out,
     decay, query, key_new, value_new, gain, inverse,
-    xbuf, wk, wv, acc, cosine, sine, weight, mini_own, mini_got, send_state, send_read, got_state, got_read,
+    xbuf, weights, acc, cosine, sine, weight, mini_own, mini_got, send_state, send_read, got_state, got_read,
     small_sem, mine_sem, sib_sem, w_sem, wl_sem, mini_sem,
     link_send, sib_send, x_send, w_send, wz_send, wzz_send, mini_send,
     tail_send, tail_send2, tail_recv, tail_recv2, chain,
@@ -125,8 +142,8 @@
 
     @pl.when(is_native)
     def _():
-        pltpu.make_async_copy(wk_hbm, wk, wl_sem.at[0]).start()
-        pltpu.make_async_copy(wv_hbm, wv, wl_sem.at[1]).start()
+        pltpu.make_async_copy(wk_hbm, weights.at[0], wl_sem.at[0]).start()
+        pltpu.make_async_copy(wv_hbm, weights.at[1], wl_sem.at[1]).start()
 
     pl.semaphore_wait(barrier, len(near))
 
@@ -176,8 +193,8 @@
     def add_product(part, mask, j, native_part, first=False):
         wrows = weight_rows(column_of(mask, native_part))
         block_x = xbuf[part, mask, piece(j), :]
-        for i, w in enumerate((wk, wv)):
-            product = jnp.dot(block_x, w[wrows, :], preferred_element_type=jnp.float32)
+        for i in range(2):
+            product = jnp.dot(block_x, weights[i, wrows, :], preferred_element_type=jnp.float32)
             if first:
                 acc[i, piece(j), :] = product
             else:
@@ -217,8 +234,8 @@
         fill_mini()
         mini_got[...] = mini_own[...]
         tables(mini_got)
-        arrived(wk, wl_sem.at[0])
-        arrived(wv, wl_sem.at[1])
+        arrived(weights.at[0], wl_sem.at[0])
+        arrived(weights.at[1], wl_sem.at[1])
         for j in range(N):
             add_product(0, 0, j, True, first=True)
         for slot in range(7):
@@ -235,18 +252,15 @@
         for j in range(N):
             sib_arrived(0, j)
             add_product(1, 0, j, False)
-        for slot in range(7):
-            k, r = FOREIGN_ORDER[slot]
-            for j in range(N):
-                sib_arrived(landing(k, r, j), j)
-                add_product(1, landing(k, r, j), j, False)
+        for k, r, j in FOREIGN_ORDER:
+            sib_arrived(landing(k, r, j), j)
+            add_product(1, landing(k, r, j), j, False)
         chain_wait(3)
 
     @pl.when(is_foreign)
     def _():
         quarter = z % 4
         opposite = (z + 2) % 4
-        kv = ((wk_hbm, wk), (wv_hbm, wv))
 
         other = flip1(x)
         mine_first = (x, 3 - x, other, 3 - other)
@@ -255,53 +269,60 @@
         def direct(row, i):
             t = row * 4 + theirs_first[i]
             rows = weight_rows(t)
-            for n, (src, dst) in enumerate(kv):
-                remote(src.at[rows], dst.at[rows], w_send, w_sem.at[t, n], partner).start()
-
-        def pass_weights(t, i, step, semaphore):
-            ref = kv[i][1]
-            rows = weight_rows(t)
-            remote(ref.at[rows], ref.at[rows], semaphore, w_sem.at[t, i], along_z(step)).start()
+            for n, src in enumerate((wk_hbm, wv_hbm)):
+                remote(src.at[rows], weights.at[n, rows], w_send, w_sem.at[t], partner).start()
+
+        def pass_weights(t, step, semaphore):
+            ref = weights.at[:, weight_rows(t)]
+            remote(ref, ref, semaphore, w_sem.at[t], along_z(step)).start()
 
         def exchange(j):
             remote(x_hbm.at[piece(j)], xbuf.at[0, 0, piece(j)], x_send, mine_sem.at[0, j], partner).start()
 
+        def send_messages(messages):
+            for k, r, j in messages:
+                send_on(turn(r, j), j, [(j + k) % N])
+
         def own_piece(j):
             mine_arrived(0, j)
-            send_on(0, j, [j])
+            send_messages(OWN_SENDS[j])
             to_sibling(0, j)
 
-        def receive(k, r, j, *to):
+        waiting = list(FOREIGN_ORDER)
+        ready = []
+
+        def receive(*expected):
+            k, r, j = waiting.pop(0)
+            assert (k, r, j) == expected
             mask = landing(k, r, j)
             mine_arrived(mask, j)
-            send_on(mask, j, [(j + kk) % N for kk in to])
+            send_messages(SENDS.get((k, r, j), []))
             to_sibling(mask, j)
+            ready.append((mask, j))
+
+        def foreign_product(count):
+            for _ in range(count):
+                mask, j = ready.pop(0)
+                add_product(0, mask, j, False)
 
         def native_product(slot):
             for j, _, mask, _ in native_slot(slot):
                 sib_arrived(mask, j)
                 add_product(1, mask, j, True)
 
-        def foreign_product(k, r):
-            for j in range(N):
-                add_product(0, landing(k, r, j), j, False)
-
         def weights_arrived(t):
-            for i, (_, ref) in enumerate(kv):
-                arrived(ref.at[weight_rows(t)], w_sem.at[t, i])
+            arrived(weights.at[:, weight_rows(t)], w_sem.at[t])
 
         def own_weights(i):
             t = quarter * 4 + mine_first[i]
             weights_arrived(t)
-            for n in range(2):
-                pass_weights(t, n, 1, wz_send)
-                pass_weights(t, n, -1, wz_send)
+            pass_weights(t, 1, wz_send)
+            pass_weights(t, -1, wz_send)
 
         def pass_on(step):
             t = (z + step) % 4 * 4 + mine_first[1 if step == 1 else 0]
             weights_arrived(t)
-            pass_weights(t, 0, -step, wzz_send)
-            pass_weights(t, 1, -step, wzz_send)
+            pass_weights(t, -step, wzz_send)
 
         def row_weights(step, *indices):
             for i in indices:
@@ -325,62 +346,60 @@
         own_piece(0)
         pass_on(-1)
         own_piece(1)
-        send_on(0, 0, [1])
         pass_on(1)
         own_piece(2)
-        send_on(0, 1, [2])
-        send_on(0, 2, [0])
         chain_wait(1)
         chain_signal(2)
         arrived(mini_got, mini_sem)
         tables(mini_got)
-        receive(0, 0, 0, 1)
+        receive(0, 0, 0)
+        own_weights(2)
+        receive(0, 0, 1)
         row_weights(1, 0)
         row_weights(3, 1)
         row_weights(2, 0, 1)
+        receive(1, 0, 2)
+        receive(0, 0, 2)
+        chain_wait(2)
+        chain_signal(3)
         for j in range(N):
             sib_arrived(0, j)
             add_product(1, 0, j, True, first=True)
-        own_weights(2)
         native_product(0)
-        receive(0, 0, 1, 1)
         native_product(1)
+        own_weights(3)
+        receive(1, 0, 0)
+        receive(2, 0, 1)
+        receive(1, 0, 1)
         native_product(2)
-        own_weights(3)
-        receive(0, 0, 2, 1)
-        for j in range(N):
-            send_on(0, j, [(j + 2) % N])
-            send_on(landing(0, 0, j), j, [(j + 2) % N])
-        chain_wait(2)
-        chain_signal(3)
         native_product(3)
         native_product(4)
-        for j in (2, 0, 1):
-            receive(1, 0, j, 2)
+        receive(1, 1, 0)
+        receive(2, 1, 1)
+        receive(2, 0, 0)
         native_product(5)
         native_product(6)
-        for j in range(N):
-            receive(1, 1, j, 2)
-        for j in range(N):
-            receive(2, 0, j)
+        receive(2, 0, 2)
+        receive(1, 1, 2)
+        receive(1, 1, 1)
+        receive(2, 1, 2)
         row_weights(1, 2, 3)
         row_weights(3, 2, 3)
         row_weights(2, 2, 3)
         for j in range(N):
             add_product(0, 0, j, False)
-        foreign_product(0, 0)
-        foreign_product(1, 0)
-        for j in range(N):
-            receive(2, 1, j)
-        foreign_product(1, 1)
-        foreign_product(2, 0)
-        for j in range(N):
-            receive(2, 2, j)
-        foreign_product(2, 1)
-        foreign_product(2, 2)
-        for j in range(N):
-            receive(2, 3, j)
-        foreign_product(2, 3)
+        foreign_product(4)
+        receive(2, 2, 1)
+        receive(2, 1, 0)
+        foreign_product(6)
+        receive(2, 2, 2)
+        receive(2, 2, 0)
+        foreign_product(5)
+        receive(2, 3, 1)
+        foreign_product(3)
+        receive(2, 3, 2)
+        receive(2, 3, 0)
+        foreign_product(3)
         chain_wait(3)
 
     scale = 128 ** (-0.5)
@@ -471,9 +490,9 @@
         arrived(got_read, tail_send2)
         arrived(xbuf.at[0, 0], x_send)
         arrived(mini_own, mini_send)
-        arrived(wk.at[pl.ds(0, 3072)], w_send)
-        arrived(wk, wz_send)
-        arrived(wk.at[pl.ds(0, 1024)], wzz_send)
+        arrived(weights.at[:, pl.ds(0, 1536)], w_send)
+        arrived(weights.at[0], wz_send)
+        arrived(weights.at[0, pl.ds(0, 1024)], wzz_send)
 
 
 def on_device(
@@ -503,8 +522,7 @@
             pltpu.VMEM((1, 256), jnp.float32),
             pltpu.VMEM((1, 128), jnp.float32),
             pltpu.VMEM((2, 8, TOK, FEAT), jnp.bfloat16),
-            pltpu.VMEM((4096, 256), jnp.bfloat16),
-            pltpu.VMEM((4096, 256), jnp.bfloat16),
+            pltpu.VMEM((2, 4096, 256), jnp.bfloat16),
             pltpu.VMEM((2, TOK, 256), jnp.float32),
             pltpu.VMEM((TOK, 128), jnp.float32),
             pltpu.VMEM((TOK, 128), jnp.float32),
@@ -515,7 +533,7 @@
             pltpu.VMEM((2, 128), jnp.float32),
             pltpu.VMEM((SP, 8, 128), jnp.bfloat16),
             pltpu.VMEM((SP, 2, 128), jnp.float32),
-            dma((6,)), dma((8, N)), dma((8, N)), dma((16, 2)), dma((2,)), dma,
+            dma((6,)), dma((8, N)), dma((8, N)), dma((16,)), dma((2,)), dma,
             dma, dma, dma, dma, dma, dma, dma,
             dma, dma, dma, dma,
             pltpu.SemaphoreType.REGULAR((4,)),

time: 59.2 us -> 56.5 us (0.954)
  Pallas kernels: 57.3 us -> 54.6 us
    pallas_call x1, Pallas kernels: 57.3 us -> 54.6 us  [on_device(): pl.pallas_call(kernel, name='gather_project_reduce', out_shape=(pltpu.VME...]
where the time goes in v6:
time: 56.5 us; the launch traced here: 56.4 us
  Pallas kernels  54.6 us (97%)
  other arithmetic  1.16 us (2%)
  between operations  0.64 us (1%)
    pallas_call x1, Pallas kernels, on_device(): pl.pallas_call(kernel, name='gather_project_reduce', out_shape=(pltpu.VME...  54.6 us

profile of v6, /device:TPU:1, one launch (start us, length us, event | category | flops | bytes accessed | tf_op | source)
XLA Modules:
  0.0 56.4 jit_solution(2539182725199116602)
XLA Ops:
  0.6 54.6 %gather_project_reduce.1 = (f32[2,8,128]{2,1,0:T(8,128)S(1)}, f32[2,256]{1,0:T(2,128)S(1)}) custom-call(f32[1,2]{1,0:T(1,128)} %bitcast.5, bf16[1024,256]{1,0:T(8,128)(2,1)} %x_hbm.1, bf16[4096,256]{1,0:T(8,128)(2,1)} %wk_hbm.1, bf16[4096,256]{1,0:T(8,128)(2,1)} %wv_hbm.1, bf16[2,256]{1,0:T(2,128)(2,1)} %query_hbm.1, bf16[2,256]{1,0:T(2,128)(2,1)} %key_hbm.1, ...), custom_call_target="tpu_custom_call" | custom-call | tf_op jit(solution)/shard_map/gather_project_reduce/pallas_call | solution.py:506
  55.3 0.6 %convert_element_type.9 = bf16[2,8,128]{2,1,0:T(8,128)(2,1)} convert(f32[2,8,128]{2,1,0:T(8,128)S(1)} %get-tuple-element.4) | non-fusion elementwise | flops 2048 | bytes 12288 | tf_op jit(solution)/shard_map/convert_element_type | solution.py:547
  55.9 0.6 convert_element_type.11

commit v7 on v6

--- a/solution.py
+++ b/solution.py
@@ -10,24 +10,24 @@
 N = 3
 TOK = 1024
 FEAT = 256
-STARTS = (0, 352, 688, 1024)
+STARTS = (0, 336, 672, 1024)
 SP = 32
 Z = 16
 
 NATIVE_ORDER = [(0, 0), (1, 0), (2, 0), (1, 1), (2, 1), (2, 2), (2, 3)]
 FOREIGN_ORDER = [
-    (0, 0, 0), (0, 0, 1), (1, 0, 2), (0, 0, 2), (1, 0, 0), (2, 0, 1), (1, 0, 1), (1, 1, 0), (2, 1, 1), (2, 0, 0),
-    (2, 0, 2), (1, 1, 2), (1, 1, 1), (2, 1, 2), (2, 2, 1), (2, 1, 0), (2, 2, 2), (2, 2, 0), (2, 3, 1), (2, 3, 2),
+    (0, 0, 0), (0, 0, 1), (1, 0, 2), (0, 0, 2), (1, 0, 0), (2, 0, 1), (1, 0, 1), (1, 1, 0), (2, 1, 1), (1, 1, 1),
+    (2, 0, 2), (1, 1, 2), (2, 0, 0), (2, 1, 2), (2, 2, 1), (2, 1, 0), (2, 2, 2), (2, 2, 0), (2, 3, 2), (2, 3, 1),
     (2, 3, 0),
 ]
 OWN_SENDS = [
     [(0, 0, 0)],
     [(0, 0, 1), (1, 0, 0)],
-    [(0, 0, 2), (1, 0, 1), (1, 0, 2), (2, 0, 1), (2, 0, 0)],
+    [(0, 0, 2), (1, 0, 1), (1, 0, 2), (2, 0, 1)],
 ]
 SENDS = {
     (0, 0, 0): [(1, 1, 0), (2, 0, 2)],
-    (0, 0, 1): [(1, 1, 1), (2, 1, 1), (2, 1, 0)],
+    (0, 0, 1): [(1, 1, 1), (2, 0, 0), (2, 1, 1), (2, 1, 0)],
     (0, 0, 2): [(1, 1, 2), (2, 1, 2)],
 }
 for _j in range(N):
@@ -83,7 +83,7 @@
     decay_hbm, x_hbm, wk_hbm, wv_hbm, query_hbm, key_hbm, value_hbm, gain_hbm, inverse_hbm,
     state_out, read_out,
     decay, query, key_new, value_new, gain, inverse,
-    xbuf, weights, acc, cosine, sine, weight, mini_own, mini_got, send_state, send_read, got_state, got_read,
+    xbuf, weights, acc, state, cosine, sine, weight, mini_own, mini_got, send_state, send_read, got_state, got_read,
     small_sem, mine_sem, sib_sem, w_sem, wl_sem, mini_sem,
     link_send, sib_send, x_send, w_send, wz_send, wzz_send, mini_send,
     tail_send, tail_send2, tail_recv, tail_recv2, chain,
@@ -121,7 +121,7 @@
     is_foreign = core != group
 
     barrier = pltpu.get_barrier_semaphore()
-    near = links + [sibling, partner, along_z(1), along_z(-1), along_z(2), along_z(-2)]
+    near = links + [sibling, partner, along_z(1), along_z(-1)]
     for device in near:
         signal(barrier, device)
 
@@ -155,10 +155,11 @@
             mini_own[2 + 2 * h : 4 + 2 * h, :] = query[:, h * 128 : h * 128 + 128].astype(jnp.float32)
 
     steps = [
-        [sibling, partner, along_z(1), along_z(-1), along_z(2), along_z(-2)],
+        [sibling, partner, along_z(1), along_z(-1)],
         [along_z(2), along_z(-2)],
         [sibling],
-        [along_z(4), along_z(-4)],
+        [along_z(3), along_z(-3)],
+        [along_z(6), along_z(-6)],
     ]
 
     def chain_signal(n):
@@ -199,6 +200,25 @@
                 acc[i, piece(j), :] = product
             else:
                 acc[i, piece(j), :] += product
+
+    scale = 128 ** (-0.5)
+
+    def add_state(j, first=False):
+        rows = piece(j)
+        for h in range(2):
+            cols = pl.ds(h * 128, 128)
+            k = acc[0, rows, cols]
+            turned = k * cosine[rows, :] + pltpu.roll(k, 64, axis=1) * sine[rows, :]
+            keys = (turned * scale).astype(jnp.bfloat16)
+            weighted = (keys.astype(jnp.float32) * weight[h, rows, :]).astype(jnp.bfloat16)
+            values = acc[1, rows, cols].astype(jnp.bfloat16)
+            part = lax.dot_general(
+                weighted, values, (((0,), (0,)), ((), ())), preferred_element_type=jnp.float32
+            )
+            if first:
+                state[h] = part
+            else:
+                state[h] += part
 
     def mine_arrived(mask, j):
         arrived(xbuf.at[0, mask, piece(j)], mine_sem.at[mask, j])
@@ -252,10 +272,15 @@
         for j in range(N):
             sib_arrived(0, j)
             add_product(1, 0, j, False)
-        for k, r, j in FOREIGN_ORDER:
+        for n, (k, r, j) in enumerate(FOREIGN_ORDER):
+            if n == 10:
+                chain_wait(3)
+                chain_signal(4)
             sib_arrived(landing(k, r, j), j)
             add_product(1, landing(k, r, j), j, False)
-        chain_wait(3)
+            if (k, r) == (2, 3):
+                add_state(j, first=j == 2)
+        chain_wait(4)
 
     @pl.when(is_foreign)
     def _():
@@ -376,12 +401,14 @@
         native_product(4)
         receive(1, 1, 0)
         receive(2, 1, 1)
-        receive(2, 0, 0)
+        receive(1, 1, 1)
         native_product(5)
         native_product(6)
+        chain_wait(3)
+        chain_signal(4)
         receive(2, 0, 2)
         receive(1, 1, 2)
-        receive(1, 1, 1)
+        receive(2, 0, 0)
         receive(2, 1, 2)
         row_weights(1, 2, 3)
         row_weights(3, 2, 3)
@@ -394,28 +421,19 @@
         foreign_product(6)
         receive(2, 2, 2)
         receive(2, 2, 0)
-        foreign_product(5)
+        foreign_product(8)
+        receive(2, 3, 2)
         receive(2, 3, 1)
-        foreign_product(3)
-        receive(2, 3, 2)
         receive(2, 3, 0)
-        foreign_product(3)
-        chain_wait(3)
-
-    scale = 128 ** (-0.5)
-    states = []
-    for h in range(2):
-        cols = pl.ds(h * 128, 128)
-        k = acc[0, :, cols]
-        turned = k * cosine[...] + pltpu.roll(k, 64, axis=1) * sine[...]
-        keys = (turned * scale).astype(jnp.bfloat16)
-        weighted = (keys.astype(jnp.float32) * weight[h]).astype(jnp.bfloat16)
-        values = acc[1, :, cols].astype(jnp.bfloat16)
-        states.append(
-            lax.dot_general(
-                weighted, values, (((0,), (0,)), ((), ())), preferred_element_type=jnp.float32
-            )
-        )
+        foreign_product(1)
+        add_state(2, first=True)
+        foreign_product(1)
+        add_state(1)
+        foreign_product(1)
+        add_state(0)
+        chain_wait(4)
+
+    states = [state[0], state[1]]
     top = lax.broadcasted_iota(jnp.int32, (8, 128), 0) < 4
     for i in range(16):
         a = states[0][8 * i : 8 * i + 8]
@@ -524,6 +542,7 @@
             pltpu.VMEM((2, 8, TOK, FEAT), jnp.bfloat16),
             pltpu.VMEM((2, 4096, 256), jnp.bfloat16),
             pltpu.VMEM((2, TOK, 256), jnp.float32),
+            pltpu.VMEM((2, 128, 128), jnp.float32),
             pltpu.VMEM((TOK, 128), jnp.float32),
             pltpu.VMEM((TOK, 128), jnp.float32),
             pltpu.VMEM((2, TOK, 128), jnp.float32),
@@ -536,7 +555,7 @@
             dma((6,)), dma((8, N)), dma((8, N)), dma((16,)), dma((2,)), dma,
             dma, dma, dma, dma, dma, dma, dma,
             dma, dma, dma, dma,
-            pltpu.SemaphoreType.REGULAR((4,)),
+            pltpu.SemaphoreType.REGULAR((5,)),
         ],
         compiler_params=pltpu.CompilerParams(collective_id=0, has_side_effects=True),
     )(

time: 56.5 us -> 56.6 us (level)
  no operation moved by 1% of the time
where the time goes in v7:
time: 56.6 us; the launch traced here: 56.5 us
  Pallas kernels  54.7 us (97%)
  other arithmetic  1.16 us (2%)
  between operations  0.64 us (1%)
    pallas_call x1, Pallas kernels, on_device(): pl.pallas_call(kernel, name='gather_project_reduce', out_shape=(pltpu.VME...  54.7 us

profile of v7, /device:TPU:1, one launch (start us, length us, event | category | flops | bytes accessed | tf_op | source)
XLA Modules:
  0.0 56.5 jit_solution(5057225134871988556)
XLA Ops:
  0.6 54.7 %gather_project_reduce.1 = (f32[2,8,128]{2,1,0:T(8,128)S(1)}, f32[2,256]{1,0:T(2,128)S(1)}) custom-call(f32[1,2]{1,0:T(1,128)} %bitcast.5, bf16[1024,256]{1,0:T(8,128)(2,1)} %x_hbm.1, bf16[4096,256]{1,0:T(8,128)(2,1)} %wk_hbm.1, bf16[4096,256]{1,0:T(8,128)(2,1)} %wv_hbm.1, bf16[2,256]{1,0:T(2,128)(2,1)} %query_hbm.1, bf16[2,256]{1,0:T(2,128)(2,1)} %key_hbm.1, ...), custom_call_target="tpu_custom_call" | custom-call | tf_op jit(solution)/shard_map/gather_project_reduce/pallas_call | solution.py:524
  55.4 0.6 %convert_element_type.9 = bf16[2,8,128]{2,1,0:T(8,128)(2,1)} convert(f32[2,8,128]{2,1,0:T(8,128)S(1)} %get-tuple-element.4) | non-fusion elementwise | flops 2048 | bytes 12288 | tf_op jit(solution)/shard_map/convert_element_type | solution.py:566
  56.0 0.6 convert_element_type.11

commit v8 on v6

--- a/solution.py
+++ b/solution.py
@@ -10,24 +10,28 @@
 N = 3
 TOK = 1024
 FEAT = 256
-STARTS = (0, 352, 688, 1024)
+STARTS = (0, 336, 672, 1024)
 SP = 32
 Z = 16
 
 NATIVE_ORDER = [(0, 0), (1, 0), (2, 0), (1, 1), (2, 1), (2, 2), (2, 3)]
 FOREIGN_ORDER = [
-    (0, 0, 0), (0, 0, 1), (1, 0, 2), (0, 0, 2), (1, 0, 0), (2, 0, 1), (1, 0, 1), (1, 1, 0), (2, 1, 1), (2, 0, 0),
-    (2, 0, 2), (1, 1, 2), (1, 1, 1), (2, 1, 2), (2, 2, 1), (2, 1, 0), (2, 2, 2), (2, 2, 0), (2, 3, 1), (2, 3, 2),
+    (0, 0, 0), (0, 0, 1), (1, 0, 2), (0, 0, 2), (1, 0, 0), (2, 0, 1), (1, 0, 1), (1, 1, 0), (2, 1, 1), (1, 1, 1),
+    (2, 0, 2), (1, 1, 2), (2, 0, 0), (2, 1, 2), (2, 2, 1), (2, 1, 0), (2, 2, 2), (2, 2, 0), (2, 3, 2), (2, 3, 1),
     (2, 3, 0),
 ]
+BATCHES = []
+for _size in (2, 2, 3, 3, 2, 2, 2, 2, 3):
+    _first = sum(len(batch) for batch in BATCHES)
+    BATCHES.append(FOREIGN_ORDER[_first : _first + _size])
 OWN_SENDS = [
     [(0, 0, 0)],
     [(0, 0, 1), (1, 0, 0)],
-    [(0, 0, 2), (1, 0, 1), (1, 0, 2), (2, 0, 1), (2, 0, 0)],
+    [(0, 0, 2), (1, 0, 1), (1, 0, 2), (2, 0, 1)],
 ]
 SENDS = {
     (0, 0, 0): [(1, 1, 0), (2, 0, 2)],
-    (0, 0, 1): [(1, 1, 1), (2, 1, 1), (2, 1, 0)],
+    (0, 0, 1): [(1, 1, 1), (2, 0, 0), (2, 1, 1), (2, 1, 0)],
     (0, 0, 2): [(1, 1, 2), (2, 1, 2)],
 }
 for _j in range(N):
@@ -41,6 +45,14 @@
 
 def piece(j):
     return pl.ds(STARTS[j], STARTS[j + 1] - STARTS[j])
+
+
+HALF = 176
+
+
+def half(j, second):
+    size = STARTS[j + 1] - STARTS[j]
+    return pl.ds(STARTS[j] + HALF, size - HALF) if second else pl.ds(STARTS[j], HALF)
 
 
 def landing(k, r, j):
@@ -84,7 +96,7 @@
     state_out, read_out,
     decay, query, key_new, value_new, gain, inverse,
     xbuf, weights, acc, cosine, sine, weight, mini_own, mini_got, send_state, send_read, got_state, got_read,
-    small_sem, mine_sem, sib_sem, w_sem, wl_sem, mini_sem,
+    small_sem, mine_sem, last_sem, sib_sem, w_sem, wl_sem, mini_sem,
     link_send, sib_send, x_send, w_send, wz_send, wzz_send, mini_send,
     tail_send, tail_send2, tail_recv, tail_recv2, chain,
 ):
@@ -121,7 +133,7 @@
     is_foreign = core != group
 
     barrier = pltpu.get_barrier_semaphore()
-    near = links + [sibling, partner, along_z(1), along_z(-1), along_z(2), along_z(-2)]
+    near = links + [sibling, partner, along_z(1), along_z(-1)]
     for device in near:
         signal(barrier, device)
 
@@ -137,15 +149,11 @@
             (gain_hbm, gain), (inverse_hbm, inverse),
         ))
     ]
-    for copy in smalls:
-        copy.start()
-
-    @pl.when(is_native)
-    def _():
-        pltpu.make_async_copy(wk_hbm, weights.at[0], wl_sem.at[0]).start()
-        pltpu.make_async_copy(wv_hbm, weights.at[1], wl_sem.at[1]).start()
-
     pl.semaphore_wait(barrier, len(near))
+
+    def start_smalls():
+        for copy in smalls:
+            copy.start()
 
     def fill_mini():
         for copy in smalls:
@@ -155,10 +163,11 @@
             mini_own[2 + 2 * h : 4 + 2 * h, :] = query[:, h * 128 : h * 128 + 128].astype(jnp.float32)
 
     steps = [
-        [sibling, partner, along_z(1), along_z(-1), along_z(2), along_z(-2)],
+        [sibling, partner, along_z(1), along_z(-1)],
         [along_z(2), along_z(-2)],
         [sibling],
-        [along_z(4), along_z(-4)],
+        [along_z(3), along_z(-3)],
+        [along_z(6), along_z(-6)],
     ]
 
     def chain_signal(n):
@@ -175,9 +184,9 @@
                 link_send, mine_sem.at[mask | (1 << d), j], links[d],
             ).start()
 
-    def to_sibling(mask, j):
+    def to_sibling(mask, j, group):
         remote(
-            xbuf.at[0, mask, piece(j)], xbuf.at[1, mask, piece(j)], sib_send, sib_sem.at[mask, j], sibling
+            xbuf.at[0, mask, piece(j)], xbuf.at[1, mask, piece(j)], sib_send, sib_sem.at[group], sibling
         ).start()
 
     def column_of(mask, native_part):
@@ -203,8 +212,9 @@
     def mine_arrived(mask, j):
         arrived(xbuf.at[0, mask, piece(j)], mine_sem.at[mask, j])
 
-    def sib_arrived(mask, j):
-        arrived(xbuf.at[1, mask, piece(j)], sib_sem.at[mask, j])
+    def sib_arrived(group, pieces):
+        rows = sum(STARTS[j + 1] - STARTS[j] for j in pieces)
+        arrived(xbuf.at[1, 0, pl.ds(0, rows)], sib_sem.at[group])
 
     def tables(mini):
         @pl.loop(0, 4)
@@ -212,7 +222,7 @@
             rows = pl.ds(pl.multiple_of(c * 256, 256), 256)
             first = (block % 16) * TOK + c * 256
             position = (lax.broadcasted_iota(jnp.int32, (256, 128), 0) + first).astype(jnp.float32)
-            table = cos_sin(position, inverse[...])
+            table = cos_sin(position, inverse[...]) * 128 ** (-0.5)
             swapped = pltpu.roll(table, 64, axis=1)
             low = lax.broadcasted_iota(jnp.int32, (256, 128), 1) < 64
             cosine[rows, :] = jnp.where(low, table, swapped)
@@ -228,8 +238,11 @@
         for slot in range(3):
             for d in range(N):
                 send_on(0, (d - slot) % N, [d])
-        for j in range(N):
-            to_sibling(0, j)
+        start_smalls()
+        pltpu.make_async_copy(wk_hbm, weights.at[0], wl_sem.at[0]).start()
+        pltpu.make_async_copy(wv_hbm, weights.at[1], wl_sem.at[1]).start()
+        for j in range(N):
+            to_sibling(0, j, 0)
         chain_signal(0)
         fill_mini()
         mini_got[...] = mini_own[...]
@@ -243,19 +256,23 @@
             for j, _, mask, onward in got:
                 mine_arrived(mask, j)
                 send_on(mask, j, onward)
-                to_sibling(mask, j)
+                to_sibling(mask, j, 1 + slot)
             if slot in (1, 3, 5):
                 chain_wait(slot // 2)
                 chain_signal(slot // 2 + 1)
             for j, _, mask, _ in got:
                 add_product(0, mask, j, True)
-        for j in range(N):
-            sib_arrived(0, j)
+        sib_arrived(0, range(N))
+        for j in range(N):
             add_product(1, 0, j, False)
-        for k, r, j in FOREIGN_ORDER:
-            sib_arrived(landing(k, r, j), j)
-            add_product(1, landing(k, r, j), j, False)
-        chain_wait(3)
+        for n, batch in enumerate(BATCHES):
+            if n == 4:
+                chain_wait(3)
+                chain_signal(4)
+            sib_arrived(1 + n, [j for _, _, j in batch])
+            for k, r, j in batch:
+                add_product(1, landing(k, r, j), j, False)
+        chain_wait(4)
 
     @pl.when(is_foreign)
     def _():
@@ -266,27 +283,37 @@
         mine_first = (x, 3 - x, other, 3 - other)
         theirs_first = (other, 3 - other, x, 3 - x)
 
-        def direct(row, i):
+        from_below, from_above, early, late = 4, 5, 6, 7
+
+        def direct(row, i, role):
             t = row * 4 + theirs_first[i]
             rows = weight_rows(t)
             for n, src in enumerate((wk_hbm, wv_hbm)):
-                remote(src.at[rows], weights.at[n, rows], w_send, w_sem.at[t], partner).start()
-
-        def pass_weights(t, step, semaphore):
+                remote(src.at[rows], weights.at[n, rows], w_send, w_sem.at[role], partner).start()
+
+        def pass_weights(t, step, semaphore, role):
             ref = weights.at[:, weight_rows(t)]
-            remote(ref, ref, semaphore, w_sem.at[t], along_z(step)).start()
+            remote(ref, ref, semaphore, w_sem.at[role], along_z(step)).start()
 
         def exchange(j):
             remote(x_hbm.at[piece(j)], xbuf.at[0, 0, piece(j)], x_send, mine_sem.at[0, j], partner).start()
 
         def send_messages(messages):
             for k, r, j in messages:
-                send_on(turn(r, j), j, [(j + k) % N])
+                if (k, r) != (2, 3):
+                    send_on(turn(r, j), j, [(j + k) % N])
+                    continue
+                for second in (False, True):
+                    remote(
+                        xbuf.at[0, turn(r, j), half(j, second)], xbuf.at[0, landing(k, r, j), half(j, second)],
+                        link_send, last_sem.at[j] if second else mine_sem.at[landing(k, r, j), j],
+                        links[(j + k) % N],
+                    ).start()
 
         def own_piece(j):
             mine_arrived(0, j)
             send_messages(OWN_SENDS[j])
-            to_sibling(0, j)
+            to_sibling(0, j, 0)
 
         waiting = list(FOREIGN_ORDER)
         ready = []
@@ -295,10 +322,17 @@
             k, r, j = waiting.pop(0)
             assert (k, r, j) == expected
             mask = landing(k, r, j)
+            ready.append((mask, j))
+            if (k, r) == (2, 3):
+                return
             mine_arrived(mask, j)
             send_messages(SENDS.get((k, r, j), []))
-            to_sibling(mask, j)
-            ready.append((mask, j))
+            to_sibling(mask, j, 1 + [(k, r, j) in batch for batch in BATCHES].index(True))
+
+        def receive_half(j, second):
+            ref = xbuf.at[0, landing(2, 3, j), half(j, second)]
+            arrived(ref, last_sem.at[j] if second else mine_sem.at[landing(2, 3, j), j])
+            remote(ref, xbuf.at[1, landing(2, 3, j), half(j, second)], sib_send, sib_sem.at[9], sibling).start()
 
         def foreign_product(count):
             for _ in range(count):
@@ -306,38 +340,36 @@
                 add_product(0, mask, j, False)
 
         def native_product(slot):
-            for j, _, mask, _ in native_slot(slot):
-                sib_arrived(mask, j)
+            got = native_slot(slot)
+            sib_arrived(1 + slot, [j for j, _, _, _ in got])
+            for j, _, mask, _ in got:
                 add_product(1, mask, j, True)
 
-        def weights_arrived(t):
-            arrived(weights.at[:, weight_rows(t)], w_sem.at[t])
+        def weights_arrived(role, columns):
+            arrived(weights.at[:, pl.ds(0, columns * FEAT)], w_sem.at[role])
 
         def own_weights(i):
             t = quarter * 4 + mine_first[i]
-            weights_arrived(t)
-            pass_weights(t, 1, wz_send)
-            pass_weights(t, -1, wz_send)
+            weights_arrived(i, 1)
+            pass_weights(t, 1, wz_send, (from_below, early, late, late)[i])
+            pass_weights(t, -1, wz_send, (early, from_above, late, late)[i])
 
         def pass_on(step):
             t = (z + step) % 4 * 4 + mine_first[1 if step == 1 else 0]
-            weights_arrived(t)
-            pass_weights(t, -step, wzz_send)
-
-        def row_weights(step, *indices):
-            for i in indices:
-                weights_arrived((z + step) % 4 * 4 + mine_first[i])
-
-        direct(quarter, 0)
-        direct(quarter, 1)
+            weights_arrived(from_above if step == 1 else from_below, 1)
+            pass_weights(t, -step, wzz_send, early)
+
+        direct(quarter, 0, 0)
+        direct(quarter, 1, 1)
+        start_smalls()
         fill_mini()
         for j in range(N):
             exchange(j)
         remote(mini_own, mini_got, mini_send, mini_sem, partner).start()
-        direct(quarter, 2)
-        direct(quarter, 3)
-        direct(opposite, 2)
-        direct(opposite, 3)
+        direct(quarter, 2, 2)
+        direct(quarter, 3, 3)
+        direct(opposite, 2, late)
+        direct(opposite, 3, late)
         chain_signal(0)
         own_weights(0)
         own_weights(1)
@@ -355,15 +387,13 @@
         receive(0, 0, 0)
         own_weights(2)
         receive(0, 0, 1)
-        row_weights(1, 0)
-        row_weights(3, 1)
-        row_weights(2, 0, 1)
+        weights_arrived(early, 4)
         receive(1, 0, 2)
         receive(0, 0, 2)
         chain_wait(2)
         chain_signal(3)
-        for j in range(N):
-            sib_arrived(0, j)
+        sib_arrived(0, range(N))
+        for j in range(N):
             add_product(1, 0, j, True, first=True)
         native_product(0)
         native_product(1)
@@ -376,16 +406,16 @@
         native_product(4)
         receive(1, 1, 0)
         receive(2, 1, 1)
-        receive(2, 0, 0)
+        receive(1, 1, 1)
         native_product(5)
         native_product(6)
+        chain_wait(3)
+        chain_signal(4)
         receive(2, 0, 2)
         receive(1, 1, 2)
-        receive(1, 1, 1)
+        receive(2, 0, 0)
         receive(2, 1, 2)
-        row_weights(1, 2, 3)
-        row_weights(3, 2, 3)
-        row_weights(2, 2, 3)
+        weights_arrived(late, 6)
         for j in range(N):
             add_product(0, 0, j, False)
         foreign_product(4)
@@ -394,21 +424,21 @@
         foreign_product(6)
         receive(2, 2, 2)
         receive(2, 2, 0)
-        foreign_product(5)
+        foreign_product(8)
+        receive(2, 3, 2)
         receive(2, 3, 1)
+        receive(2, 3, 0)
+        for second in (False, True):
+            for j in (2, 1, 0):
+                receive_half(j, second)
         foreign_product(3)
-        receive(2, 3, 2)
-        receive(2, 3, 0)
-        foreign_product(3)
-        chain_wait(3)
-
-    scale = 128 ** (-0.5)
+        chain_wait(4)
+
     states = []
     for h in range(2):
         cols = pl.ds(h * 128, 128)
         k = acc[0, :, cols]
-        turned = k * cosine[...] + pltpu.roll(k, 64, axis=1) * sine[...]
-        keys = (turned * scale).astype(jnp.bfloat16)
+        keys = (k * cosine[...] + pltpu.roll(k, 64, axis=1) * sine[...]).astype(jnp.bfloat16)
         weighted = (keys.astype(jnp.float32) * weight[h]).astype(jnp.bfloat16)
         values = acc[1, :, cols].astype(jnp.bfloat16)
         states.append(
@@ -493,6 +523,11 @@
         arrived(weights.at[:, pl.ds(0, 1536)], w_send)
         arrived(weights.at[0], wz_send)
         arrived(weights.at[0, pl.ds(0, 1024)], wzz_send)
+
+
+def round_results(state, read, state_out, read_out):
+    state_out[...] = state[...].astype(jnp.bfloat16)
+    read_out[...] = read[...].astype(jnp.bfloat16)
 
 
 def on_device(
@@ -533,20 +568,28 @@
             pltpu.VMEM((2, 128), jnp.float32),
             pltpu.VMEM((SP, 8, 128), jnp.bfloat16),
             pltpu.VMEM((SP, 2, 128), jnp.float32),
-            dma((6,)), dma((8, N)), dma((8, N)), dma((16,)), dma((2,)), dma,
+            dma((6,)), dma((8, N)), dma((N,)), dma((10,)), dma((8,)), dma((2,)), dma,
             dma, dma, dma, dma, dma, dma, dma,
             dma, dma, dma, dma,
-            pltpu.SemaphoreType.REGULAR((4,)),
+            pltpu.SemaphoreType.REGULAR((5,)),
         ],
         compiler_params=pltpu.CompilerParams(collective_id=0, has_side_effects=True),
     )(
         decay_exponent[None, :], layer_input, key_weight, value_weight,
         query_new, key_new, value_new, norm_gain[None, :], inverse,
     )
-    return (
-        state.reshape(2, 2, 4, 128).astype(jnp.bfloat16),
-        read.astype(jnp.bfloat16),
-    )
+    in_vmem = [pltpu.with_memory_space_constraint(result, pltpu.VMEM) for result in (state, read)]
+    state, read = pl.pallas_call(
+        round_results,
+        name="round_results",
+        out_shape=(
+            jax.ShapeDtypeStruct((2, 8, 128), jnp.bfloat16),
+            jax.ShapeDtypeStruct((2, 256), jnp.bfloat16),
+        ),
+        in_specs=[vmem, vmem],
+        out_specs=(vmem, vmem),
+    )(*in_vmem)
+    return (state.reshape(2, 2, 4, 128), read)
 
 
 def solution(mesh):

time: 56.5 us -> 54.8 us (0.970)
  other arithmetic: 1.16 us -> 0 us
  Pallas kernels: 54.6 us -> 54 us
    pallas_call x1, Pallas kernels: 54.6 us -> 53.4 us  [on_device(): pl.pallas_call(kernel, name='gather_project_reduce', out_shape=(pltpu.VME...]
    convert_element_type x2 -> x0, other arithmetic: 1.16 us -> none  [the longest x1 0.6 us: on_device(): state.reshape(2, 2, 4, 128).astype(jnp.bfloat16)]
    pallas_call x0 -> x1, Pallas kernels: none -> 0.6 us  [on_device(): pl.pallas_call(round_results, name='round_results', out_shape=(jax.ShapeD...]
where the time goes in v8:
time: 54.8 us; the launch traced here: 54.7 us
  Pallas kernels  54 us (99%)
  between operations  0.64 us (1%)
    pallas_call x1, Pallas kernels, on_device(): pl.pallas_call(kernel, name='gather_project_reduce', out_shape=(pltpu.VME...  53.4 us

profile of v8, /device:TPU:1, one launch (start us, length us, event | category | flops | bytes accessed | tf_op | source)
XLA Modules:
  0.0 54.7 jit_solution(13546303770343888893)
XLA Ops:
  0.6 53.4 %gather_project_reduce.1 = (f32[2,8,128]{2,1,0:T(8,128)S(1)}, f32[2,256]{1,0:T(2,128)S(1)}) custom-call(f32[1,2]{1,0:T(1,128)} %bitcast.4, bf16[1024,256]{1,0:T(8,128)(2,1)} %x_hbm.1, bf16[4096,256]{1,0:T(8,128)(2,1)} %wk_hbm.1, bf16[4096,256]{1,0:T(8,128)(2,1)} %wv_hbm.1, bf16[2,256]{1,0:T(2,128)(2,1)} %query_hbm.1, bf16[2,256]{1,0:T(2,128)(2,1)} %key_hbm.1, ...), custom_call_target="tpu_custom_call" | custom-call | tf_op jit(solution)/shard_map/gather_project_reduce/pallas_call | solution.py:541
  54.1 0.6 %round_results.1 = (bf16[2,8,128]{2,1,0:T(8,128)(2,1)}, bf16[2,256]{1,0:T(2,128)(2,1)}) custom-call(f32[2,8,128]{2,1,0:T(8,128)S(1)} %get-tuple-element.6.state, f32[2,256]{1,0:T(2,128)S(1)} %get-tuple-element.7.read), custom_call_target="tpu_custom_call" | custom-call | tf_op jit(solution)/shard_map/round_results/pallas_call | solution.py:582

commit v9 on v8

--- a/solution.py
+++ b/solution.py
@@ -95,7 +95,7 @@
     decay_hbm, x_hbm, wk_hbm, wv_hbm, query_hbm, key_hbm, value_hbm, gain_hbm, inverse_hbm,
     state_out, read_out,
     decay, query, key_new, value_new, gain, inverse,
-    xbuf, weights, acc, cosine, sine, weight, mini_own, mini_got, send_state, send_read, got_state, got_read,
+    xbuf, weights, acc, state, cosine, sine, weight, mini_own, mini_got, send_state, send_read, got_state, got_read,
     small_sem, mine_sem, last_sem, sib_sem, w_sem, wl_sem, mini_sem,
     link_send, sib_send, x_send, w_send, wz_send, wzz_send, mini_send,
     tail_send, tail_send2, tail_recv, tail_recv2, chain,
@@ -199,15 +199,31 @@
     def weight_rows(t):
         return pl.ds(pl.multiple_of(t * FEAT, FEAT), FEAT)
 
-    def add_product(part, mask, j, native_part, first=False):
+    def add_product(part, mask, j, native_part, first=False, second=None):
         wrows = weight_rows(column_of(mask, native_part))
-        block_x = xbuf[part, mask, piece(j), :]
+        rows = piece(j) if second is None else half(j, second)
+        block_x = xbuf[part, mask, rows, :]
         for i in range(2):
             product = jnp.dot(block_x, weights[i, wrows, :], preferred_element_type=jnp.float32)
             if first:
-                acc[i, piece(j), :] = product
+                acc[i, rows, :] = product
             else:
-                acc[i, piece(j), :] += product
+                acc[i, rows, :] += product
+
+    def add_state(ranges, first=False):
+        for h in range(2):
+            cols = pl.ds(h * 128, 128)
+            total = None if first else state[h]
+            for rows in ranges:
+                k = acc[0, rows, cols]
+                keys = (k * cosine[rows, :] + pltpu.roll(k, 64, axis=1) * sine[rows, :]).astype(jnp.bfloat16)
+                weighted = (keys.astype(jnp.float32) * weight[h, rows, :]).astype(jnp.bfloat16)
+                values = acc[1, rows, cols].astype(jnp.bfloat16)
+                product = lax.dot_general(
+                    weighted, values, (((0,), (0,)), ((), ())), preferred_element_type=jnp.float32
+                )
+                total = product if total is None else total + product
+            state[h] = total
 
     def mine_arrived(mask, j):
         arrived(xbuf.at[0, mask, piece(j)], mine_sem.at[mask, j])
@@ -269,9 +285,18 @@
             if n == 4:
                 chain_wait(3)
                 chain_signal(4)
+            if n == 8:
+                continue
             sib_arrived(1 + n, [j for _, _, j in batch])
             for k, r, j in batch:
                 add_product(1, landing(k, r, j), j, False)
+        for second in (False, True):
+            ranges = [half(j, second) for j in (2, 1, 0)]
+            rows = sum(span.size for span in ranges)
+            arrived(xbuf.at[1, 0, pl.ds(0, rows)], sib_sem.at[10 if second else 9])
+            for j in (2, 1, 0):
+                add_product(1, landing(2, 3, j), j, False, second=second)
+            add_state(ranges, first=not second)
         chain_wait(4)
 
     @pl.when(is_foreign)
@@ -332,7 +357,7 @@
         def receive_half(j, second):
             ref = xbuf.at[0, landing(2, 3, j), half(j, second)]
             arrived(ref, last_sem.at[j] if second else mine_sem.at[landing(2, 3, j), j])
-            remote(ref, xbuf.at[1, landing(2, 3, j), half(j, second)], sib_send, sib_sem.at[9], sibling).start()
+            remote(ref, xbuf.at[1, landing(2, 3, j), half(j, second)], sib_send, sib_sem.at[10 if second else 9], sibling).start()
 
         def foreign_product(count):
             for _ in range(count):
@@ -424,28 +449,20 @@
         foreign_product(6)
         receive(2, 2, 2)
         receive(2, 2, 0)
-        foreign_product(8)
+        foreign_product(4)
         receive(2, 3, 2)
         receive(2, 3, 1)
         receive(2, 3, 0)
-        for second in (False, True):
-            for j in (2, 1, 0):
-                receive_half(j, second)
+        for j in (2, 1, 0):
+            receive_half(j, False)
+        foreign_product(4)
+        for j in (2, 1, 0):
+            receive_half(j, True)
         foreign_product(3)
+        add_state([pl.ds(0, TOK)], first=True)
         chain_wait(4)
 
-    states = []
-    for h in range(2):
-        cols = pl.ds(h * 128, 128)
-        k = acc[0, :, cols]
-        keys = (k * cosine[...] + pltpu.roll(k, 64, axis=1) * sine[...]).astype(jnp.bfloat16)
-        weighted = (keys.astype(jnp.float32) * weight[h]).astype(jnp.bfloat16)
-        values = acc[1, :, cols].astype(jnp.bfloat16)
-        states.append(
-            lax.dot_general(
-                weighted, values, (((0,), (0,)), ((), ())), preferred_element_type=jnp.float32
-            )
-        )
+    states = [state[0], state[1]]
     top = lax.broadcasted_iota(jnp.int32, (8, 128), 0) < 4
     for i in range(16):
         a = states[0][8 * i : 8 * i + 8]
@@ -453,10 +470,14 @@
         send_state[2 * i] = jnp.where(top, a, pltpu.roll(b, 4, axis=0)).astype(jnp.bfloat16)
         send_state[2 * i + 1] = jnp.where(top, pltpu.roll(a, 4, axis=0), b).astype(jnp.bfloat16)
     prompt = z // 8
+    reads = []
     for h in range(2):
         rows = pl.ds(2 + 2 * h, 2)
-        both = jnp.dot(mini_got[rows, :], states[h], precision=lax.Precision.HIGHEST, preferred_element_type=jnp.float32)
-        send_read[h : h + 1, :] = jnp.where(prompt == 0, both[0:1], both[1:2])
+        both = jnp.dot(
+            mini_got[rows, :], states[h], precision=lax.Precision.HIGHEST, preferred_element_type=jnp.float32
+        )
+        reads.append(jnp.where(prompt == 0, both[0:1], both[1:2]))
+    send_read[...] = jnp.concatenate(reads, axis=0).astype(jnp.bfloat16)
 
     target_tp = jnp.where(is_native, tp, partner_tp)
 
@@ -492,7 +513,7 @@
     ]
 
     arrived(got_read, tail_recv2)
-    carried = [jnp.sum(got_read[16 * s : 16 * s + 16], axis=0) for s in range(2)]
+    carried = [jnp.sum(got_read[16 * s : 16 * s + 16].astype(jnp.float32), axis=0) for s in range(2)]
     for h in range(2):
         scaled = jnp.exp(mini_own[h : h + 1, :])
         rows = jnp.concatenate([carried[0][h : h + 1], carried[1][h : h + 1]], axis=0)
@@ -559,16 +580,17 @@
             pltpu.VMEM((2, 8, TOK, FEAT), jnp.bfloat16),
             pltpu.VMEM((2, 4096, 256), jnp.bfloat16),
             pltpu.VMEM((2, TOK, 256), jnp.float32),
+            pltpu.VMEM((2, 128, 128), jnp.float32),
             pltpu.VMEM((TOK, 128), jnp.float32),
             pltpu.VMEM((TOK, 128), jnp.float32),
             pltpu.VMEM((2, TOK, 128), jnp.float32),
             pltpu.VMEM((8, 128), jnp.float32),
             pltpu.VMEM((8, 128), jnp.float32),
             pltpu.VMEM((SP, 8, 128), jnp.bfloat16),
-            pltpu.VMEM((2, 128), jnp.float32),
+            pltpu.VMEM((2, 128), jnp.bfloat16),
             pltpu.VMEM((SP, 8, 128), jnp.bfloat16),
-            pltpu.VMEM((SP, 2, 128), jnp.float32),
-            dma((6,)), dma((8, N)), dma((N,)), dma((10,)), dma((8,)), dma((2,)), dma,
+            pltpu.VMEM((SP, 2, 128), jnp.bfloat16),
+            dma((6,)), dma((8, N)), dma((N,)), dma((11,)), dma((8,)), dma((2,)), dma,
             dma, dma, dma, dma, dma, dma, dma,
             dma, dma, dma, dma,
             pltpu.SemaphoreType.REGULAR((5,)),

time: 54.8 us -> 54.2 us (0.989)
    pallas_call x1, Pallas kernels: 53.4 us -> 52.9 us  [on_device(): pl.pallas_call(kernel, name='gather_project_reduce', out_shape=(pltpu.VME...]
where the time goes in v9:
time: 54.2 us; the launch traced here: 54.1 us
  Pallas kernels  53.5 us (99%)
  between operations  0.64 us (1%)
    pallas_call x1, Pallas kernels, on_device(): pl.pallas_call(kernel, name='gather_project_reduce', out_shape=(pltpu.VME...  52.9 us

profile of v9, /device:TPU:1, one launch (start us, length us, event | category | flops | bytes accessed | tf_op | source)
XLA Modules:
  0.0 54.1 jit_solution(1806434483519928089)
XLA Ops:
  0.6 52.9 %gather_project_reduce.1 = (f32[2,8,128]{2,1,0:T(8,128)S(1)}, f32[2,256]{1,0:T(2,128)S(1)}) custom-call(f32[1,2]{1,0:T(1,128)} %bitcast.4, bf16[1024,256]{1,0:T(8,128)(2,1)} %x_hbm.1, bf16[4096,256]{1,0:T(8,128)(2,1)} %wk_hbm.1, bf16[4096,256]{1,0:T(8,128)(2,1)} %wv_hbm.1, bf16[2,256]{1,0:T(2,128)(2,1)} %query_hbm.1, bf16[2,256]{1,0:T(2,128)(2,1)} %key_hbm.1, ...), custom_call_target="tpu_custom_call" | custom-call | tf_op jit(solution)/shard_map/gather_project_reduce/pallas_call | solution.py:562
  53.5 0.6 %round_results.1 = (bf16[2,8,128]{2,1,0:T(8,128)(2,1)}, bf16[2,256]{1,0:T(2,128)(2,1)}) custom-call(f32[2,8,128]{2,1,0:T(8,128)S(1)} %get-tuple-element.6.state, f32[2,256]{1,0:T(2,128)S(1)} %get-tuple-element.7.read), custom_call_target="tpu_custom_call" | custom-call | tf_op jit(solution)/shard_map/round_results/pallas_call | solution.py:604

commit v10 on v9

--- a/solution.py
+++ b/solution.py
@@ -48,6 +48,7 @@
 
 
 HALF = 176
+ROWS = 10
 
 
 def half(j, second):
@@ -95,10 +96,10 @@
     decay_hbm, x_hbm, wk_hbm, wv_hbm, query_hbm, key_hbm, value_hbm, gain_hbm, inverse_hbm,
     state_out, read_out,
     decay, query, key_new, value_new, gain, inverse,
-    xbuf, weights, acc, state, cosine, sine, weight, mini_own, mini_got, send_state, send_read, got_state, got_read,
+    xbuf, weights, acc, state, cosine, sine, weight, mini_own, mini_got, send_share, got_share,
     small_sem, mine_sem, last_sem, sib_sem, w_sem, wl_sem, mini_sem,
     link_send, sib_send, x_send, w_send, wz_send, wzz_send, mini_send,
-    tail_send, tail_send2, tail_recv, tail_recv2, chain,
+    tail_send, tail_recv, chain,
 ):
     sp = lax.axis_index("sp")
     tp = lax.axis_index("tp")
@@ -463,12 +464,6 @@
         chain_wait(4)
 
     states = [state[0], state[1]]
-    top = lax.broadcasted_iota(jnp.int32, (8, 128), 0) < 4
-    for i in range(16):
-        a = states[0][8 * i : 8 * i + 8]
-        b = states[1][8 * i : 8 * i + 8]
-        send_state[2 * i] = jnp.where(top, a, pltpu.roll(b, 4, axis=0)).astype(jnp.bfloat16)
-        send_state[2 * i + 1] = jnp.where(top, pltpu.roll(a, 4, axis=0), b).astype(jnp.bfloat16)
     prompt = z // 8
     reads = []
     for h in range(2):
@@ -477,15 +472,26 @@
             mini_got[rows, :], states[h], precision=lax.Precision.HIGHEST, preferred_element_type=jnp.float32
         )
         reads.append(jnp.where(prompt == 0, both[0:1], both[1:2]))
-    send_read[...] = jnp.concatenate(reads, axis=0).astype(jnp.bfloat16)
+    reads = jnp.concatenate(reads + [jnp.zeros((6, 128), jnp.float32)], axis=0)
+    top = lax.broadcasted_iota(jnp.int32, (8, 128), 0) < 4
+    for i in range(16):
+        a = states[0][8 * i : 8 * i + 8]
+        b = states[1][8 * i : 8 * i + 8]
+        for n, share in enumerate((
+            jnp.where(top, a, pltpu.roll(b, 4, axis=0)), jnp.where(top, pltpu.roll(a, 4, axis=0), b)
+        )):
+            send_share[2 * i + n] = jnp.concatenate([share, reads], axis=0).astype(jnp.bfloat16)
 
     target_tp = jnp.where(is_native, tp, partner_tp)
+
+    sent = pl.ds(0, ROWS)
 
     def tail(step, other):
         target = (z + step + Z) % Z * 2 + (1 - core if other else core)
         device = (target, target_tp)
-        remote(send_state.at[target], got_state.at[block], tail_send, tail_recv, device).start()
-        remote(send_read, got_read.at[block], tail_send2, tail_recv2, device).start()
+        remote(
+            send_share.at[target, sent], got_share.at[block, sent], tail_send, tail_recv, device
+        ).start()
 
     far = [8]
     for s in range(7, 0, -1):
@@ -497,8 +503,7 @@
 
     @pl.when(is_native)
     def _():
-        pltpu.make_async_copy(send_state.at[sp], got_state.at[block], tail_recv).start()
-        pltpu.make_async_copy(send_read, got_read.at[block], tail_recv2).start()
+        pltpu.make_async_copy(send_share.at[sp, sent], got_share.at[block, sent], tail_recv).start()
 
     @pl.when(is_foreign)
     def _():
@@ -512,19 +517,18 @@
         for h in range(2)
     ]
 
-    arrived(got_read, tail_recv2)
-    carried = [jnp.sum(got_read[16 * s : 16 * s + 16].astype(jnp.float32), axis=0) for s in range(2)]
+    arrived(got_share.at[:, sent], tail_recv)
+    carried = [jnp.sum(got_share[16 * s : 16 * s + 16, 8:10, :].astype(jnp.float32), axis=0) for s in range(2)]
     for h in range(2):
         scaled = jnp.exp(mini_own[h : h + 1, :])
         rows = jnp.concatenate([carried[0][h : h + 1], carried[1][h : h + 1]], axis=0)
         mixed = scaled * rows + own_terms[h]
         normed = mixed * lax.rsqrt(jnp.mean(mixed * mixed, axis=1, keepdims=True) + 1e-06)
         read_out[:, h * 128 : h * 128 + 128] = normed * gain[:, h * 128 : h * 128 + 128]
-    arrived(got_state, tail_recv)
     for s in range(2):
         total = jnp.zeros((8, 128), jnp.float32)
         for i in range(16):
-            total = total + got_state[16 * s + i].astype(jnp.float32)
+            total = total + got_share[16 * s + i, 0:8, :].astype(jnp.float32)
         state_out[s] = total
 
     arrived(xbuf.at[0, pl.ds(0, 7)], link_send)
@@ -532,13 +536,11 @@
 
     @pl.when(is_native)
     def _():
-        arrived(got_state.at[pl.ds(0, 31)], tail_send)
-        arrived(got_read.at[pl.ds(0, 31)], tail_send2)
+        arrived(got_share.at[pl.ds(0, 31), sent], tail_send)
 
     @pl.when(is_foreign)
     def _():
-        arrived(got_state, tail_send)
-        arrived(got_read, tail_send2)
+        arrived(got_share.at[:, sent], tail_send)
         arrived(xbuf.at[0, 0], x_send)
         arrived(mini_own, mini_send)
         arrived(weights.at[:, pl.ds(0, 1536)], w_send)
@@ -586,13 +588,11 @@
             pltpu.VMEM((2, TOK, 128), jnp.float32),
             pltpu.VMEM((8, 128), jnp.float32),
             pltpu.VMEM((8, 128), jnp.float32),
-            pltpu.VMEM((SP, 8, 128), jnp.bfloat16),
-            pltpu.VMEM((2, 128), jnp.bfloat16),
-            pltpu.VMEM((SP, 8, 128), jnp.bfloat16),
-            pltpu.VMEM((SP, 2, 128), jnp.bfloat16),
+            pltpu.VMEM((SP, 16, 128), jnp.bfloat16),
+            pltpu.VMEM((SP, 16, 128), jnp.bfloat16),
             dma((6,)), dma((8, N)), dma((N,)), dma((11,)), dma((8,)), dma((2,)), dma,
             dma, dma, dma, dma, dma, dma, dma,
-            dma, dma, dma, dma,
+            dma, dma,
             pltpu.SemaphoreType.REGULAR((5,)),
         ],
         compiler_params=pltpu.CompilerParams(collective_id=0, has_side_effects=True),

time: 54.2 us -> 54.1 us (level)
  no operation moved by 1% of the time
where the time goes in v10:
time: 54.1 us; the launch traced here: 54 us
  Pallas kernels  53.3 us (99%)
  between operations  0.64 us (1%)
    pallas_call x1, Pallas kernels, on_device(): pl.pallas_call(kernel, name='gather_project_reduce', out_shape=(pltpu.VME...  52.7 us

profile of v10, /device:TPU:1, one launch (start us, length us, event | category | flops | bytes accessed | tf_op | source)
XLA Modules:
  0.0 54.0 jit_solution(13746751798894232086)
XLA Ops:
  0.6 52.7 %gather_project_reduce.1 = (f32[2,8,128]{2,1,0:T(8,128)S(1)}, f32[2,256]{1,0:T(2,128)S(1)}) custom-call(f32[1,2]{1,0:T(1,128)} %bitcast.4, bf16[1024,256]{1,0:T(8,128)(2,1)} %x_hbm.1, bf16[4096,256]{1,0:T(8,128)(2,1)} %wk_hbm.1, bf16[4096,256]{1,0:T(8,128)(2,1)} %wv_hbm.1, bf16[2,256]{1,0:T(2,128)(2,1)} %query_hbm.1, bf16[2,256]{1,0:T(2,128)(2,1)} %key_hbm.1, ...), custom_call_target="tpu_custom_call" | custom-call | tf_op jit(solution)/shard_map/gather_project_reduce/pallas_call | solution.py:564
  53.4 0.6 %round_results.1 = (bf16[2,8,128]{2,1,0:T(8,128)(2,1)}, bf16[2,256]{1,0:T(2,128)(2,1)}) custom-call(f32[2,8,128]{2,1,0:T(8,128)S(1)} %get-tuple-element.6.state, f32[2,256]{1,0:T(2,128)S(1)} %get-tuple-element.7.read), custom_call_target="tpu_custom_call" | custom-call | tf_op jit(solution)/shard_map/round_results/pallas_call | solution.py:604

commit v11 on v10

--- a/solution.py
+++ b/solution.py
@@ -468,9 +468,12 @@
     reads = []
     for h in range(2):
         rows = pl.ds(2 + 2 * h, 2)
-        both = jnp.dot(
-            mini_got[rows, :], states[h], precision=lax.Precision.HIGHEST, preferred_element_type=jnp.float32
-        )
+        q = mini_got[rows, :].astype(jnp.bfloat16)
+        high = states[h].astype(jnp.bfloat16)
+        rest = states[h] - high.astype(jnp.float32)
+        middle = rest.astype(jnp.bfloat16)
+        low = (rest - middle.astype(jnp.float32)).astype(jnp.bfloat16)
+        both = sum(jnp.dot(q, part, preferred_element_type=jnp.float32) for part in (low, middle, high))
         reads.append(jnp.where(prompt == 0, both[0:1], both[1:2]))
     reads = jnp.concatenate(reads + [jnp.zeros((6, 128), jnp.float32)], axis=0)
     top = lax.broadcasted_iota(jnp.int32, (8, 128), 0) < 4

time: 54.1 us -> 54.1 us (level)
  no operation moved by 1% of the time
where the time goes in v11:
time: 54.1 us; the launch traced here: 53.9 us
  Pallas kernels  53.3 us (99%)
  between operations  0.64 us (1%)
    pallas_call x1, Pallas kernels, on_device(): pl.pallas_call(kernel, name='gather_project_reduce', out_shape=(pltpu.VME...  52.7 us

profile of v11, /device:TPU:1, one launch (start us, length us, event | category | flops | bytes accessed | tf_op | source)
XLA Modules:
  0.0 53.9 jit_solution(724157121025549357)
XLA Ops:
  0.6 52.7 %gather_project_reduce.1 = (f32[2,8,128]{2,1,0:T(8,128)S(1)}, f32[2,256]{1,0:T(2,128)S(1)}) custom-call(f32[1,2]{1,0:T(1,128)} %bitcast.4, bf16[1024,256]{1,0:T(8,128)(2,1)} %x_hbm.1, bf16[4096,256]{1,0:T(8,128)(2,1)} %wk_hbm.1, bf16[4096,256]{1,0:T(8,128)(2,1)} %wv_hbm.1, bf16[2,256]{1,0:T(2,128)(2,1)} %query_hbm.1, bf16[2,256]{1,0:T(2,128)(2,1)} %key_hbm.1, ...), custom_call_target="tpu_custom_call" | custom-call | tf_op jit(solution)/shard_map/gather_project_reduce/pallas_call | solution.py:567
  53.3 0.6 %round_results.1 = (bf16[2,8,128]{2,1,0:T(8,128)(2,1)}, bf16[2,256]{1,0:T(2,128)(2,1)}) custom-call(f32[2,8,128]{2,1,0:T(8,128)S(1)} %get-tuple-element.6.state, f32[2,256]{1,0:T(2,128)S(1)} %get-tuple-element.7.read), custom_call_target="tpu_custom_call" | custom-call | tf_op jit(solution)/shard_map/round_results/pallas_call | solution.py:607
